TPU v7x, 256 devices: a whole 4x4x8 slice. The times are simulated.
256 devices in a mesh: fs: 32 (over z, y), tp: 8 (over x, core).
Axes of the slice: x: 4, y: 4, z: 8, core: 2. Of those that a mesh axis runs over, the one named last changes fastest.
Arguments:
- prompt: bfloat16 [24576, 2048], P('fs'), may hold values from -6 to 6
- routes: int32 [24576, 2], P('fs'), may hold values from 0 to 63, all different within a row; in each aligned block of 768 rows (0 to 767, 768 to 1535, ...) at most 48 rows name the same one
- affinity: float32 [24576, 2], P('fs'), may hold values from 0.05 to 1
- norm_gain: float32 [2048], P('fs'), may hold values from 0.1 to 1.9
- gate_master: float32 [64, 2048, 1024], P(None, 'fs', 'tp'), may hold values from -0.125 to 0.125
- up_master: float32 [64, 2048, 1024], P(None, 'fs', 'tp'), may hold values from -0.125 to 0.125
- down_master: float32 [64, 1024, 2048], P(None, 'fs', 'tp'), may hold values from -0.1875 to 0.1875
Outputs:
- mixed: bfloat16 [24576, 2048], P('fs', 'tp')
- gate_weights: bfloat16 [64, 2048, 1024], P('fs', None, 'tp')
- up_weights: bfloat16 [64, 2048, 1024], P('fs', None, 'tp')
- down_weights: bfloat16 [64, 1024, 2048], P('fs', None, 'tp')
Inputs may be any that keep to these rules, and one draw needn't show every extreme that they name: `routes`: each row names 2 different experts. In each aligned block of 768 rows no expert is named more than 48 times, a bound that some block reaches.
All inputs are finite; a program needn't handle non-finite values.
Results may differ from a plain program's by a relative error of at most 0.0086.
Values may be sent and summed in bfloat16 or wider, within the bound.
No kernel may reach another device: no remote copies, remote signals or barrier semaphores. Data moves between devices by JAX's collectives and lax.ppermute only.
A program may use at most 128 MiB of HBM per device.

v0:
```python
import jax
import jax.numpy as jnp
from jax import lax
from jax.sharding import PartitionSpec as P

norm_eps = 1e-06


def side_by_side(arrays, axis, split_dim, concat_dim, along):
    widths = [a.shape[along] for a in arrays]
    both = jnp.concatenate(arrays, axis=along)
    whole = lax.all_to_all(both, axis, split_axis=split_dim, concat_axis=concat_dim, tiled=True)
    return tuple(jnp.split(whole, [sum(widths[:k]) for k in range(1, len(widths))], axis=along))


def per_device(prompt, routes, affinity, norm_gain, gate_master, up_master, down_master):
    tp_count = lax.axis_size("tp")
    experts = gate_master.shape[0]
    gain_rows = norm_gain[None, :, None]
    gate_half = (gate_master * gain_rows).astype(jnp.bfloat16)
    up_half = (up_master * gain_rows).astype(jnp.bfloat16)
    down_half = down_master.astype(jnp.bfloat16)
    gate_new, up_new, down_new = (
        *side_by_side((gate_half, up_half), "fs", 0, 1, 2),
        lax.all_to_all(down_half, "fs", split_axis=0, concat_axis=1, tiled=True),
    )
    token_count = prompt.shape[0]
    top_count = routes.shape[1]
    model_width = prompt.shape[1]
    capacity = 2 * token_count * top_count // experts
    flat_ids = routes.reshape(-1)
    onehot = (flat_ids[:, None] == jnp.arange(experts, dtype=jnp.int32)[None, :]).astype(jnp.int32)
    slot_rank = jnp.sum(jnp.cumsum(onehot, axis=0) * onehot, axis=1) - 1
    slot_index = flat_ids * capacity + slot_rank
    values = prompt.astype(jnp.float32)
    normed = (
        values * lax.rsqrt(jnp.mean(values * values, axis=-1, keepdims=True) + norm_eps)
    ).astype(jnp.bfloat16)
    column_width = model_width // tp_count
    column_slice = lax.dynamic_slice_in_dim(
        normed, lax.axis_index("tp") * column_width, column_width, 1
    )
    slot_rows = jnp.broadcast_to(
        column_slice[:, None, :], (token_count, top_count, column_width)
    ).reshape(-1, column_width)
    outbox = (
        jnp.zeros((experts * capacity, column_width), jnp.bfloat16).at[slot_index].set(slot_rows)
    )
    received = lax.all_to_all(
        outbox.reshape(experts, capacity, column_width),
        "fs",
        split_axis=0,
        concat_axis=1,
        tiled=True,
    )
    shard_piece = lax.all_gather(received, "tp", axis=2, tiled=True)
    gate_pre = jnp.einsum("erd,edf->erf", shard_piece, gate_new, preferred_element_type=jnp.float32)
    up_pre = jnp.einsum("erd,edf->erf", shard_piece, up_new, preferred_element_type=jnp.float32)
    hidden = (jax.nn.silu(gate_pre) * up_pre).astype(jnp.bfloat16)
    expert_out = jnp.einsum(
        "erf,efd->erd",
        lax.all_gather(hidden, "tp", axis=2, tiled=True),
        down_new,
        preferred_element_type=jnp.float32,
    ).astype(jnp.bfloat16)
    returned = lax.all_to_all(expert_out, "fs", split_axis=1, concat_axis=0, tiled=True)
    picked = returned.reshape(experts * capacity, -1)[slot_index].reshape(
        token_count, top_count, -1
    )
    share = affinity / jnp.sum(affinity, axis=1, keepdims=True)
    mixed_out = jnp.sum(share[:, :, None] * picked.astype(jnp.float32), axis=1).astype(jnp.bfloat16)
    return (mixed_out, gate_new, up_new, down_new)


def solution(mesh):
    in_specs = (
        P("fs", None),
        P("fs", None),
        P("fs", None),
        P("fs"),
        P(None, "fs", "tp"),
        P(None, "fs", "tp"),
        P(None, "fs", "tp"),
    )
    out_specs = (P("fs", "tp"), P("fs", None, "tp"), P("fs", None, "tp"), P("fs", None, "tp"))
    return jax.shard_map(
        per_device, mesh=mesh, in_specs=in_specs, out_specs=out_specs, check_vma=False
    )
```

profile of v0, /device:TPU:16, one launch (start us, length us, event | category | flops | bytes accessed | tf_op | source)
XLA Modules:
  0.0 310.5 jit_solution(14779207124408148616)
XLA Ops:
  7.2 5.5 %convert_element_type.36 = f32[768,2048]{1,0:T(8,128)} convert(bf16[768,2048]{1,0:T(8,128)(2,1)} %param.7) | non-fusion elementwise | flops 1572864 | bytes 9437184 | tf_op jit(solution)/shard_map/convert_element_type | solution.py:35
  12.8 0.7 multiply_reduce_fusion
  13.7 0.2 eq.29
  14.1 1.3 fusion.1
  15.5 0.4 broadcast_in_dim.5
  15.9 0.3 reshape.101
  16.2 18.1 %reduce-window.6 = s32[64,12,128]{2,1,0:T(8,128)S(1)} reduce-window(s32[64,12,128]{2,1,0:T(8,128)S(1)} %fusion.4, s32[]{:T(128)} %constant.15.clone.1), window={size=1x1x128 pad=0_0x0_0x127_0}, to_apply=%region_1.2 | reduce-window | flops 12484608 | bytes 786436 | tf_op jit(solution)/shard_map/reduce-window
  34.6 0.3 copy.29
  35.5 0.3 mul.65
  35.8 7.6 %scatter_custom_fusion = bf16[3072,256]{1,0:T(8,128)(2,1)S(1)} fusion(s32[1536]{0:T(1024)S(1)} %fusion.7, bf16[1536,256]{1,0:T(8,128)(2,1)S(1)} %reshape.101, bf16[]{:T(256)} %constant.13.clone.1), kind=kCustom, calls=%fused_computation.12 | custom fusion | bytes 1572866 | tf_op jit(solution)/shard_map/scatter | solution.py:47
  43.5 50.7 %all_to_all.69 = bf16[64,48,256]{2,1,0:T(8,128)(2,1)S(1)} all-to-all(bf16[64,48,256]{2,1,0:T(8,128)(2,1)S(1)} %bitcast.43), channel_id=1, replica_groups=mesh['fs'=32,'tp'=8] {'fs'}, dimensions={0} | all-to-all | bytes 3145728 | tf_op jit(solution)/shard_map/all_to_all | solution.py:49
  94.2 1.3 copy.31
  95.5 0.8 copy-done.3
  96.3 2.2 multiply_convert_fusion.1
  98.5 0.3 pad_maximum_fusion
  98.8 55.1 %all_to_all.70 = bf16[64,64,256]{2,1,0:T(8,128)(2,1)S(1)} all-to-all(bf16[64,64,256]{2,1,0:T(8,128)(2,1)S(1)} %pad_maximum_fusion), channel_id=1, replica_groups=mesh['fs'=32,'tp'=8] {'fs'}, dimensions={0} | all-to-all | bytes 4194304 | tf_op jit(solution)/shard_map/all_to_all | solution.py:12
  154.0 0.2 copy.32
  154.2 0.4 fusion.8
  154.6 11.9 %all-gather.3.cloned.1.call-done = bf16[2,1536,2048]{2,1,0:T(8,128)(2,1)} async-done(((bf16[2,1536,256]{2,1,0:T(8,128)(2,1)}), bf16[2,1536,2048]{2,1,0:T(8,128)(2,1)}) %all-gather.3.cloned.1.call-update) | async-done | bytes 12582928 | tf_op jit(solution)/shard_map/all_gather | solution.py:56
  166.5 7.8 %fusion.9 = f32[2,1536,128]{2,1,0:T(8,128)S(1)} fusion(bf16[2,1536,2048]{2,1,0:T(8,128)(2,1)} %all-gather.3.cloned.1.call-done, bf16[2,2048,128]{2,1,0:T(8,128)(2,1)S(1)} %get-tuple-element.4), kind=kOutput, calls=%fused_computation.29 | convolution fusion | flops 1610612736 | bytes 15204352 | tf_op jit(solution)/shard_map/erd,edf->erf/dot_general | solution.py:57
  174.3 0.4 copy-done.1
  174.7 4.7 %fusion = bf16[2,1536,128]{2,1,0:T(8,128)(2,1)} fusion(bf16[2,1536,2048]{2,1,0:T(8,128)(2,1)S(1)} %copy-done.1, bf16[2,2048,128]{2,1,0:T(8,128)(2,1)S(1)} %get-tuple-element.5, f32[2,1536,128]{2,1,0:T(8,128)S(1)} %fusion.9), kind=kOutput, calls=%fused_computation.5 | convolution fusion | flops 1612972032 | bytes 15990784 | tf_op jit(solution)/shard_map/erd,edf->erf/dot_general | solution.py:58
  179.6 38.4 %all_to_all.71 = bf16[64,32,256]{2,1,0:T(8,128)(2,1)S(1)} all-to-all(bf16[64,32,256]{2,1,0:T(8,128)(2,1)S(1)} %convert_element_type.41), channel_id=1, replica_groups=mesh['fs'=32,'tp'=8] {'fs'}, dimensions={0} | all-to-all | bytes 2097152 | tf_op jit(solution)/shard_map/all_to_all | solution.py:25
  218.1 9.4 %all-gather.5.cloned.1.call-done = bf16[2,1536,1024]{2,1,0:T(8,128)(2,1)} async-done(((bf16[2,1536,128]{2,1,0:T(8,128)(2,1)}), bf16[2,1536,1024]{2,1,0:T(8,128)(2,1)}) %all-gather.5.cloned.1.call-update) | async-done | bytes 6291472 | tf_op jit(solution)/shard_map/all_gather | solution.py:62
  227.5 4.6 %convolution_convert_fusion = bf16[2,1536,256]{2,1,0:T(8,128)(2,1)S(1)} fusion(bf16[2,1536,1024]{2,1,0:T(8,128)(2,1)} %all-gather.5.cloned.1.call-done, bf16[2,1024,256]{2,1,0:T(8,128)(2,1)S(1)} %bitcast.47), kind=kOutput, calls=%fused_computation.3 | convolution fusion | flops 1611399168 | bytes 8912896 | tf_op jit(solution)/shard_map/erf,efd->erd/dot_general | solution.py:60
  232.1 10.7 %copy.34 = bf16[2,1536,256]{2,0,1:T(2,128)(2,1)} copy(bf16[2,1536,256]{2,1,0:T(8,128)(2,1)S(1)} %convolution_convert_fusion) | data formatting | bytes 3145728 | tf_op jit(solution)/shard_map/convert_element_type | solution.py:65
  242.8 10.3 %all-to-all-start.3 = ((bf16[2,1536,256]{2,0,1:T(2,128)(2,1)}), bf16[2,1536,256]{2,0,1:T(2,128)(2,1)S(1)}, u32[]{:S(2)}, u32[]{:S(2)}) async-start(bf16[2,1536,256]{2,0,1:T(2,128)(2,1)} %copy.34), calls=%async_computation.3 | async-start | bytes 3145728 | tf_op jit(solution)/shard_map/all_to_all | solution.py:66
  253.4 39.5 %all-to-all-done.3 = bf16[2,1536,256]{2,0,1:T(2,128)(2,1)S(1)} async-done(((bf16[2,1536,256]{2,0,1:T(2,128)(2,1)}), bf16[2,1536,256]{2,0,1:T(2,128)(2,1)S(1)}, u32[]{:S(2)}, u32[]{:S(2)}) %all-to-all-start.3) | async-done | bytes 1572896 | tf_op jit(solution)/shard_map/all_to_all | solution.py:66
  292.8 0.3 copy.35
  293.1 4.8 %gather_fusion = bf16[1536,256]{1,0:T(8,128)(2,1)S(1)} fusion(bf16[3072,256]{1,0:T(8,128)(2,1)S(1)} %bitcast.38, s32[2048]{0:T(1024)S(1)} %pad_clamp_fusion), kind=kCustom, calls=%fused_computation | custom fusion | bytes 1579008 | tf_op jit(solution)/shard_map/gather | solution.py:67
  297.9 0.8 reshape.88
  298.7 5.0 %multiply_reduce_fusion.1 = bf16[768,256]{1,0:T(8,128)(2,1)} fusion(f32[768,2,256]{2,1,0:T(2,128)S(1)} %reshape.88, f32[768,2]{1,0:T(8,128)S(1)} %copy.25), kind=kLoop, calls=%fused_computation.9 | loop fusion | flops 589824 | bytes 1972224 | tf_op jit(solution)/shard_map/reduce_sum | solution.py:71
  (41 shorter events, 2.0 us)
Async XLA Ops:
  7.2 159.4 %all-gather.3.cloned.1.call-start = ((), (), s32[]{:S(2)}) async-start(), calls=%async_computation.4 | async-start | bytes 14155776 | tf_op jit(solution)/shard_map/all_gather | solution.py:56
  7.2 5.6 %copy-start = (bf16[768,2048]{1,0:T(8,128)(2,1)S(1)}, bf16[768,2048]{1,0:T(8,128)(2,1)}, u32[]{:S(2)}) copy-start(bf16[768,2048]{1,0:T(8,128)(2,1)} %param.7) | copy-start | bytes 9437188
  12.8 0.7 copy-start.8
  94.2 2.2 copy-start.3
  94.2 2.2 copy-start.9
  95.5 132.0 %all-gather.5.cloned.1.call-start = ((), (), s32[]{:S(2)}) async-start(), calls=%async_computation.5 | async-start | bytes 7077888 | tf_op jit(solution)/shard_map/all_gather | solution.py:62
  154.6 19.7 %copy-start.2 = (bf16[2,2048,128]{2,1,0:T(8,128)(2,1)}, bf16[2,2048,128]{2,1,0:T(8,128)(2,1)S(1)}, u32[]{:S(2)}) copy-start(bf16[2,2048,128]{2,1,0:T(8,128)(2,1)S(1)} %get-tuple-element.4) | copy-start | bytes 3145732
  154.6 19.7 %copy-start.6 = (bf16[2,2048,128]{2,1,0:T(8,128)(2,1)}, bf16[2,2048,128]{2,1,0:T(8,128)(2,1)S(1)}, u32[]{:S(2)}) copy-start(bf16[2,2048,128]{2,1,0:T(8,128)(2,1)S(1)} %get-tuple-element.5) | copy-start | bytes 3145732
  166.5 8.2 %copy-start.1 = (bf16[2,1536,2048]{2,1,0:T(8,128)(2,1)S(1)}, bf16[2,1536,2048]{2,1,0:T(8,128)(2,1)}, u32[]{:S(2)}) copy-start(bf16[2,1536,2048]{2,1,0:T(8,128)(2,1)} %all-gather.3.cloned.1.call-done) | copy-start | bytes 37748740
  174.7 4.7 %copy-start.4 = (f32[64,32,256]{2,1,0:T(8,128)S(1)}, f32[64,32,256]{2,1,0:T(8,128)}, u32[]{:S(2)}) copy-start(f32[64,32,256]{2,1,0:T(8,128)} %param.13) | copy-start | bytes 6291460
  218.1 14.0 %copy-start.5 = (bf16[32,2,32,256]{3,2,0,1:T(8,128)(2,1)}, bf16[32,2,32,256]{3,2,0,1:T(8,128)(2,1)S(1)}, u32[]{:S(2)}) copy-start(bf16[32,2,32,256]{3,2,0,1:T(8,128)(2,1)S(1)} %copy.33) | copy-start | bytes 3145732
  242.8 10.3 %copy-start.7 = (f32[768,2]{0,1:T(2,128)S(1)}, f32[768,2]{0,1:T(2,128)}, u32[]{:S(2)}) copy-start(f32[768,2]{0,1:T(2,128)} %param.9) | copy-start | bytes 18436
  242.8 50.0 %all-to-all-start.3 = ((bf16[2,1536,256]{2,0,1:T(2,128)(2,1)}), bf16[2,1536,256]{2,0,1:T(2,128)(2,1)S(1)}, u32[]{:S(2)}, u32[]{:S(2)}) async-start(bf16[2,1536,256]{2,0,1:T(2,128)(2,1)} %copy.34), calls=%async_computation.3 | async-start | bytes 3145728 | tf_op jit(solution)/shard_map/all_to_all | solution.py:66
Sparse Core Ops, SparseCore 0:
  95.6 70.8 all-gather.2
  179.5 47.9 all-gather.4
where the time goes:
time: 311 us
  blocking collectives  144 us (46%)
  waiting for transfers between devices  60.8 us (20%)
  other arithmetic  33.8 us (11%)
  local copies, waits for them, and re-layouts  29.9 us (10%)
  matrix products  17 us (5%)
  between operations  14.4 us (5%)
  starting transfers between devices  10.4 us (3%)
    all_to_all x1, blocking collectives, side_by_side(): lax.all_to_all(both, axis, split_axis=split_dim, concat_axis=concat_dim,...  55.1 us
    all_to_all x1, blocking collectives, per_device(): lax.all_to_all(outbox.reshape(experts, capacity, column_width), 'fs', spl...  50.7 us
    all_to_all x1, waiting for transfers between devices, per_device(): lax.all_to_all(expert_out, 'fs', split_axis=1, concat_axis=0, tiled=True)  39.5 us
    all_to_all x1, blocking collectives, per_device(): lax.all_to_all(down_half, 'fs', split_axis=0, concat_axis=1, tiled=True)  38.4 us
    another operation x3, other arithmetic  18.4 us
    all_gather x1, waiting for transfers between devices, per_device(): shard_piece = lax.all_gather(received, 'tp', axis=2, tiled=True)  11.9 us
    convert_element_type x1, local copies, waits for them, and re-layouts, per_device(): expert_out = jnp.einsum('erf,efd->erd', lax.all_gather(hidden, 'tp', axis...  10.7 us
    all_to_all x1, starting transfers between devices, per_device(): lax.all_to_all(expert_out, 'fs', split_axis=1, concat_axis=0, tiled=True)  10.3 us
  transfers between devices with their start and end apart: 3, of which 3 were waited for; matrix products, arithmetic and copies ran while one was open for 1% of the time, Pallas kernels for 0%

commit v1 on v0

v1 whole, which is shorter than its diff:
```python
import functools
import jax
import jax.numpy as jnp
from jax import lax
from jax.experimental import pallas as pl
from jax.experimental.pallas import tpu as pltpu
from jax.sharding import PartitionSpec as P

norm_eps = 1e-06
VMEM_LIMIT = 48 * 1024 * 1024


def dispatch_kernel(row_steps, cap, experts, tp_ref, routes_ref, prompt_ref, out_ref, slots_ref, normed_ref):
    step = pl.program_id(0)
    tokens = routes_ref.shape[1]
    width = normed_ref.shape[1]
    rows = prompt_ref.shape[0]

    @pl.when(step == 0)
    def _():
        ids = routes_ref[...]
        expert = lax.broadcasted_iota(jnp.int32, (experts, tokens), 0)
        hit0 = ids[0:1, :] == expert
        hit1 = ids[1:2, :] == expert
        named = jnp.where(hit0 | hit1, 1.0, 0.0).astype(jnp.bfloat16)
        earlier = lax.broadcasted_iota(jnp.int32, (tokens, tokens), 0) < lax.broadcasted_iota(
            jnp.int32, (tokens, tokens), 1
        )
        before = jnp.where(earlier, 1.0, 0.0).astype(jnp.bfloat16)
        count = jnp.dot(named, before, preferred_element_type=jnp.float32)
        rank0 = jnp.sum(jnp.where(hit0, count, 0.0), axis=0, keepdims=True).astype(jnp.int32)
        rank1 = jnp.sum(jnp.where(hit1, count, 0.0), axis=0, keepdims=True).astype(jnp.int32)
        slots_ref[0:1, :] = ids[0:1, :] * cap + rank0
        slots_ref[1:2, :] = ids[1:2, :] * cap + rank1

    @pl.when(step < row_steps)
    def _():
        values = prompt_ref[...].astype(jnp.float32)
        scale = lax.rsqrt(jnp.mean(values * values, axis=1, keepdims=True) + norm_eps)
        start = pl.multiple_of(tp_ref[0] * width, width)
        part = prompt_ref[:, pl.ds(start, width)].astype(jnp.float32)
        normed_ref[pl.ds(pl.multiple_of(step * rows, rows), rows), :] = (part * scale).astype(jnp.bfloat16)

    @pl.when(step >= row_steps)
    def _():
        block = out_ref.shape[0]
        slot = lax.broadcasted_iota(jnp.int32, (block, tokens), 0) + (step - row_steps) * block
        chosen = (slots_ref[0:1, :] == slot) | (slots_ref[1:2, :] == slot)
        out_ref[...] = jnp.dot(
            jnp.where(chosen, 1.0, 0.0).astype(jnp.bfloat16),
            normed_ref[...],
            preferred_element_type=jnp.float32,
        ).astype(jnp.bfloat16)


def dispatch(prompt, routes, tp_index, cap, experts, width):
    tokens, model_width = prompt.shape
    row_steps, slot_steps = 4, 4
    rows, block = tokens // row_steps, experts * cap // slot_steps
    return pl.pallas_call(
        functools.partial(dispatch_kernel, row_steps, cap, experts),
        grid_spec=pltpu.PrefetchScalarGridSpec(
            num_scalar_prefetch=1,
            grid=(row_steps + slot_steps,),
            in_specs=[
                pl.BlockSpec((2, tokens), lambda i, tp: (0, 0)),
                pl.BlockSpec((rows, model_width), lambda i, tp: (jnp.minimum(i, row_steps - 1), 0)),
            ],
            out_specs=[
                pl.BlockSpec((block, width), lambda i, tp: (jnp.maximum(i - row_steps, 0), 0)),
                pl.BlockSpec((2, tokens), lambda i, tp: (0, 0)),
            ],
            scratch_shapes=[pltpu.VMEM((tokens, width), jnp.bfloat16)],
        ),
        out_shape=[
            jax.ShapeDtypeStruct((experts * cap, width), jnp.bfloat16),
            jax.ShapeDtypeStruct((2, tokens), jnp.int32),
        ],
        compiler_params=pltpu.CompilerParams(
            dimension_semantics=("arbitrary",), vmem_limit_bytes=VMEM_LIMIT
        ),
        name="dispatch",
    )(tp_index, routes.T, prompt)


def combine_kernel(slots_ref, affinity_ref, rows_ref, out_ref, first_ref, second_ref):
    step = pl.program_id(0)
    tokens = slots_ref.shape[0]
    block = rows_ref.shape[0]
    slot = lax.broadcasted_iota(jnp.int32, (tokens, block), 1) + step * block
    rows = rows_ref[...]

    @pl.when(step == 0)
    def _():
        first_ref[...] = jnp.zeros_like(first_ref)
        second_ref[...] = jnp.zeros_like(second_ref)

    for k, total in ((0, first_ref), (1, second_ref)):
        chosen = jnp.where(slots_ref[:, k : k + 1] == slot, 1.0, 0.0).astype(jnp.bfloat16)
        total[...] += jnp.dot(chosen, rows, preferred_element_type=jnp.float32)

    @pl.when(step == pl.num_programs(0) - 1)
    def _():
        affinity = affinity_ref[...]
        share = affinity / jnp.sum(affinity, axis=1, keepdims=True)
        out_ref[...] = (share[:, 0:1] * first_ref[...] + share[:, 1:2] * second_ref[...]).astype(jnp.bfloat16)


def combine(slots, affinity, rows):
    tokens = affinity.shape[0]
    slot_count, width = rows.shape
    steps = 4
    block = slot_count // steps
    return pl.pallas_call(
        combine_kernel,
        grid=(steps,),
        in_specs=[
            pl.BlockSpec((tokens, 2), lambda i: (0, 0)),
            pl.BlockSpec((tokens, 2), lambda i: (0, 0)),
            pl.BlockSpec((block, width), lambda i: (i, 0)),
        ],
        out_specs=pl.BlockSpec((tokens, width), lambda i: (0, 0)),
        scratch_shapes=[pltpu.VMEM((tokens, width), jnp.float32)] * 2,
        out_shape=jax.ShapeDtypeStruct((tokens, width), jnp.bfloat16),
        compiler_params=pltpu.CompilerParams(
            dimension_semantics=("arbitrary",), vmem_limit_bytes=VMEM_LIMIT
        ),
        name="combine",
    )(slots.T, affinity, rows)


WHOLE = ((0, 0), (0, 1), (3, 0), (3, 1), (1, 0), (1, 1))
SPLIT = ((2, 0), (2, 1))


def expert_matmul_kernel(gated, half_step, tp_ref, *refs):
    whole, low, high = refs[:6], refs[6:8], refs[8:10]
    weight_ref, out_ref, total_ref = refs[10:]
    sources, _, cap, width = whole[0].shape
    rows = sources * cap
    group = weight_ref.shape[0] // 8
    step = pl.program_id(1)

    index = tp_ref[0]

    def product(piece, position):
        dx, swap = (WHOLE + SPLIT)[position]
        source = (((index >> 1) + dx) & 3) * 2 + ((index & 1) ^ swap)
        block = weight_ref[pl.ds(source * group, group), 0]
        return jnp.dot(
            piece[:, 0].reshape(rows, width),
            block.reshape(width, block.shape[-1]),
            preferred_element_type=jnp.float32,
        )

    total = product(whole[0], 0)
    for position in range(1, 6):
        total += product(whole[position], position)
    total_ref[...] = total

    @pl.when(step < half_step)
    def _():
        total_ref[...] += product(low[0], 6) + product(low[1], 7)

    @pl.when(step >= half_step)
    def _():
        total_ref[...] += product(high[0], 6) + product(high[1], 7)

    result = total_ref[...]
    if gated:
        half = result.shape[1] // 2
        gate, up = result[:, :half], result[:, half:]
        result = gate / (1.0 + jnp.exp(-gate)) * up
    out_ref[...] = result.astype(jnp.bfloat16).reshape(out_ref.shape)


def expert_matmul(pieces, weight, order, gated, out_width):
    whole, low, high = pieces
    sources, experts, cap, width = whole[0].shape
    steps = 4
    chunk = sources // steps
    half_step = steps // 2
    block = (chunk, 1, cap, width)
    rows = chunk * cap
    return pl.pallas_call(
        functools.partial(expert_matmul_kernel, gated, half_step),
        grid_spec=pltpu.PrefetchScalarGridSpec(
            num_scalar_prefetch=1,
            grid=(experts, steps),
            in_specs=[pl.BlockSpec(block, lambda e, j, o: (j, e, 0, 0))] * 6
            + [pl.BlockSpec(block, lambda e, j, o: (jnp.minimum(j, half_step - 1), e, 0, 0))] * 2
            + [pl.BlockSpec(block, lambda e, j, o: (jnp.maximum(j - half_step, 0), e, 0, 0))] * 2
            + [pl.BlockSpec((sources, 1) + weight.shape[2:], lambda e, j, o: (0, e, 0, 0))],
            out_specs=pl.BlockSpec((chunk, 1, cap, out_width), lambda e, j, o: (j, e, 0, 0)),
            scratch_shapes=[pltpu.VMEM((rows, weight.shape[-1]), jnp.float32)],
        ),
        out_shape=jax.ShapeDtypeStruct((sources, experts, cap, out_width), jnp.bfloat16),
        compiler_params=pltpu.CompilerParams(
            dimension_semantics=("arbitrary", "arbitrary"), vmem_limit_bytes=VMEM_LIMIT
        ),
    )(order, *whole, *low, *high, weight)


def tp_move(dx, swap):
    return [(2 * x + c, 2 * ((x + dx) % 4) + (c ^ swap)) for x in range(4) for c in range(2)]


def spread(own):
    half = own.shape[0] // 2
    right = lax.ppermute(own, "tp", tp_move(1, 0))
    left = lax.ppermute(own, "tp", tp_move(3, 0))
    own_other = lax.ppermute(own, "tp", tp_move(0, 1))
    low = lax.ppermute(right[:half], "tp", tp_move(1, 0))
    high = lax.ppermute(left[half:], "tp", tp_move(3, 0))
    right_other = lax.ppermute(right, "tp", tp_move(0, 1))
    left_other = lax.ppermute(left, "tp", tp_move(0, 1))
    low_other = lax.ppermute(low, "tp", tp_move(0, 1))
    high_other = lax.ppermute(high, "tp", tp_move(0, 1))
    return (own, own_other, right, right_other, left, left_other), (low, low_other), (high, high_other)


def exchange(array):
    return lax.all_to_all(array, "fs", split_axis=0, concat_axis=0, tiled=True)


def layer(prompt, routes, affinity, norm_gain, gate_master, up_master, down_master):
    fs_count, tp_count = lax.axis_size("fs"), lax.axis_size("tp")
    experts, gain_rows, hidden_width = gate_master.shape
    here = experts // fs_count
    token_count, top_count = routes.shape
    capacity = 2 * token_count * top_count // experts
    width = prompt.shape[1] // tp_count
    tp_index = lax.axis_index("tp").astype(jnp.int32)
    tp_index = tp_index.reshape(1)

    outbox, slots = dispatch(prompt, routes, tp_index, capacity, experts, width)
    received = exchange(outbox.reshape(fs_count, here, capacity, width))

    gain = norm_gain[None, :, None]
    gate_up = jnp.concatenate(
        [(gate_master * gain).astype(jnp.bfloat16), (up_master * gain).astype(jnp.bfloat16)], axis=2
    ).reshape(fs_count, here, gain_rows, 2 * hidden_width)
    down = down_master.astype(jnp.bfloat16).reshape((fs_count, here) + down_master.shape[1:])

    pieces = spread(received)
    gate_up_new = exchange(gate_up)
    hidden = expert_matmul(pieces, gate_up_new, tp_index, True, hidden_width)
    down_new = exchange(down)
    expert_out = expert_matmul(spread(hidden), down_new, tp_index, False, width)
    returned = exchange(expert_out)
    mixed = combine(slots, affinity, returned.reshape(experts * capacity, width))

    def rows_first(array):
        return array.transpose(1, 0, 2, 3).reshape(here, -1, array.shape[-1])

    return (
        mixed,
        rows_first(gate_up_new[..., :hidden_width]),
        rows_first(gate_up_new[..., hidden_width:]),
        rows_first(down_new),
    )


def solution(mesh):
    in_specs = (
        P("fs", None),
        P("fs", None),
        P("fs", None),
        P("fs"),
        P(None, "fs", "tp"),
        P(None, "fs", "tp"),
        P(None, "fs", "tp"),
    )
    out_specs = (P("fs", "tp"), P("fs", None, "tp"), P("fs", None, "tp"), P("fs", None, "tp"))
    return jax.shard_map(layer, mesh=mesh, in_specs=in_specs, out_specs=out_specs, check_vma=False)
```

time: 311 us -> 243 us (0.78)
  blocking collectives: 144 us -> 0 us
  waiting for transfers between devices: 60.8 us -> 141 us
  starting transfers between devices: 10.4 us -> 52.6 us
  Pallas kernels: 0 us -> 29.6 us
  other arithmetic: 33.8 us -> 5.74 us
  local copies, waits for them, and re-layouts: 29.9 us -> 12.6 us
  matrix products: 17 us -> 0 us
  between operations: 14.4 us -> 0.84 us
    all_to_all x3 -> x0, blocking collectives: 144 us -> none  [the longest x1 55.1 us: side_by_side(): lax.all_to_all(both, axis, split_axis=split_dim, concat_axis=concat_dim,...]
    ppermute x0 -> x18, waiting for transfers between devices: none -> 72.9 us  [the longest x2 50 us: spread(): right = lax.ppermute(own, 'tp', tp_move(1, 0))]
    pallas_call x0 -> x4, Pallas kernels: none -> 29.6 us  [the longest x2 19.9 us: expert_matmul(): pl.pallas_call(functools.partial(expert_matmul_kernel, gated, half_step),...]
    all_to_all x1 -> x4, waiting for transfers between devices: 39.5 us -> 67.9 us  [exchange(): return lax.all_to_all(array, 'fs', split_axis=0, concat_axis=0, tiled=True)]
    all_to_all x1 -> x4, starting transfers between devices: 10.3 us -> 37.1 us  [exchange(): return lax.all_to_all(array, 'fs', split_axis=0, concat_axis=0, tiled=True)]
    all_gather x2 -> x0, waiting for transfers between devices: 21.3 us -> none  [the longest x1 11.9 us: per_device(): shard_piece = lax.all_gather(received, 'tp', axis=2, tiled=True)]
    another operation x3 -> x0, other arithmetic: 18.4 us -> none
    dot_general x3 -> x0, matrix products: 17 us -> none  [the longest x1 7.76 us: per_device(): jnp.einsum('erd,edf->erf', shard_piece, gate_new, preferred_element_type=...]
  transfers between devices with their start and end apart: 3 -> 22, of which waited for: 3 -> 9; matrix products, arithmetic and copies ran while one was open for 1% -> 6% of each run, Pallas kernels for 0% -> 4%
where the time goes in v1:
time: 243 us; the launch traced here: 242 us
  waiting for transfers between devices  141 us (58%)
  starting transfers between devices  52.6 us (22%)
  Pallas kernels  29.6 us (12%)
  local copies, waits for them, and re-layouts  12.6 us (5%)
  other arithmetic  5.74 us (2%)
    all_to_all x4, waiting for transfers between devices, exchange(): return lax.all_to_all(array, 'fs', split_axis=0, concat_axis=0, tiled=True)  67.9 us
    ppermute x2, waiting for transfers between devices, spread(): right = lax.ppermute(own, 'tp', tp_move(1, 0))  50 us
    all_to_all x4, starting transfers between devices, exchange(): return lax.all_to_all(array, 'fs', split_axis=0, concat_axis=0, tiled=True)  37.1 us
    ppermute x2, waiting for transfers between devices, spread(): low = lax.ppermute(right[:half], 'tp', tp_move(1, 0))  20.5 us
    pallas_call x2, Pallas kernels, expert_matmul(): pl.pallas_call(functools.partial(expert_matmul_kernel, gated, half_step),...  19.9 us
    ppermute x2, starting transfers between devices, spread(): high = lax.ppermute(left[half:], 'tp', tp_move(3, 0))  6.32 us
    transpose x4, local copies, waits for them, and re-layouts, rows_first(): return array.transpose(1, 0, 2, 3).reshape(here, -1, array.shape[-1])  6.07 us
    pallas_call x1, Pallas kernels, combine(): pl.pallas_call(combine_kernel, grid=(steps,), in_specs=[pl.BlockSpec((tok...  5.02 us
  transfers between devices with their start and end apart: 22, of which 9 were waited for; matrix products, arithmetic and copies ran while one was open for 6% of the time, Pallas kernels for 4%

profile of v1, /device:TPU:16, one launch (start us, length us, event | category | flops | bytes accessed | tf_op | source)
XLA Modules:
  0.0 242.2 jit_solution(13926486510481457040)
XLA Ops:
  0.6 1.9 copy-done
  3.2 4.7 %dispatch.1 = (bf16[3072,256]{1,0:T(8,128)(2,1)}, s32[2,768]{1,0:T(2,128)S(1)}) custom-call(s32[1]{0:T(128)} %bitcast.tp_ref, s32[2,768]{1,0:T(2,128)S(1)} %bitcast.17, bf16[768,2048]{1,0:T(8,128)(2,1)S(1)} %copy-done), custom_call_target="tpu_custom_call" | custom-call | tf_op jit(solution)/shard_map/dispatch/pallas_call | solution.py:60
  7.9 11.7 %all-to-all-start = ((bf16[32,2,48,256]{3,2,1,0:T(8,128)(2,1)}), bf16[32,2,48,256]{3,2,1,0:T(8,128)(2,1)S(1)}, u32[]{:S(2)}, u32[]{:S(2)}) async-start(bf16[32,2,48,256]{3,2,1,0:T(8,128)(2,1)} %bitcast.3), calls=%async_computation | async-start | bytes 3145728 | tf_op jit(solution)/shard_map/all_to_all | solution.py:223
  19.7 2.9 %multiply_convert_fusion.1 = (bf16[64,64,128]{2,1,0:T(8,128)(2,1)S(1)}, bf16[64,64,128]{2,1,0:T(8,128)(2,1)S(1)}) fusion(f32[64,64,128]{2,1,0:T(8,128)} %param.11, f32[64]{0:T(128)S(1)} %copy-done.6, f32[64,64,128]{2,1,0:T(8,128)} %param.12), kind=kLoop, calls=%fused_computation.2 | loop fusion | flops 2097152 | bytes 6291712 | tf_op jit(solution)/shard_map/convert_element_type | solution.py:241
  22.5 1.7 pad_maximum_fusion
  24.2 34.8 %all-to-all-done.refs_0_ = bf16[32,2,48,256]{3,2,1,0:T(8,128)(2,1)S(1)} async-done(((bf16[32,2,48,256]{3,2,1,0:T(8,128)(2,1)}), bf16[32,2,48,256]{3,2,1,0:T(8,128)(2,1)S(1)}, u32[]{:S(2)}, u32[]{:S(2)}) %all-to-all-start) | async-done | bytes 1572896 | tf_op jit(solution)/shard_map/all_to_all | solution.py:223
  59.0 5.6 %all-to-all-start.1 = ((bf16[32,2,64,256]{3,2,1,0:T(8,128)(2,1)}), bf16[32,2,64,256]{3,2,1,0:T(8,128)(2,1)}, u32[]{:S(2)}, u32[]{:S(2)}) async-start(bf16[32,2,64,256]{3,2,1,0:T(8,128)(2,1)} %bitcast.18), calls=%async_computation.1 | async-start | bytes 4194304 | tf_op jit(solution)/shard_map/all_to_all | solution.py:223
  64.6 1.6 collective-permute-start.1
  66.2 1.7 collective-permute-start.3
  67.9 32.5 %collective-permute-done.1.refs_2_ = bf16[32,2,48,256]{3,2,1,0:T(8,128)(2,1)} collective-permute-done((bf16[32,2,48,256]{3,2,1,0:T(8,128)(2,1)S(1)}, bf16[32,2,48,256]{3,2,1,0:T(8,128)(2,1)}, u32[]{:S(2)}, u32[]{:S(2)}) %collective-permute-start.1) | collective-permute-done | bytes 1572896 | tf_op jit(solution)/shard_map/ppermute | solution.py:210
  100.4 1.2 slice.24
  102.0 1.2 slice.25
  103.2 3.0 %collective-permute-start.7 = (bf16[16,2,48,256]{3,2,1,0:T(8,128)(2,1)S(1)}, bf16[16,2,48,256]{3,2,1,0:T(8,128)(2,1)S(1)}, u32[]{:S(2)}, u32[]{:S(2)}) collective-permute-start(bf16[16,2,48,256]{3,2,1,0:T(8,128)(2,1)S(1)} %slice.25), channel_id=1, source_target_pairs={{0,6},{1,7},{2,0},{3,1},{4,2},{5,3},{6,4},{7,5},{8,14},{9,15},{10,... | collective-permute-start | bytes 2359304 | tf_op jit(solution)/shard_map/ppermute | solution.py:214
  106.7 12.9 %collective-permute-done.5.refs_6_ = bf16[16,2,48,256]{3,2,1,0:T(8,128)(2,1)S(1)} collective-permute-done((bf16[16,2,48,256]{3,2,1,0:T(8,128)(2,1)S(1)}, bf16[16,2,48,256]{3,2,1,0:T(8,128)(2,1)S(1)}, u32[]{:S(2)}, u32[]{:S(2)}) %collective-permute-start.5) | collective-permute-done | bytes 786464 | tf_op jit(solution)/shard_map/ppermute | solution.py:213
  120.2 1.2 convert_element_type.11
  121.4 9.8 %all-to-all-start.2 = ((bf16[32,2,32,256]{3,2,1,0:T(8,128)(2,1)}), bf16[32,2,32,256]{3,2,1,0:T(8,128)(2,1)}, u32[]{:S(2)}, u32[]{:S(2)}) async-start(bf16[32,2,32,256]{3,2,1,0:T(8,128)(2,1)} %bitcast.19), calls=%async_computation.2 | async-start | bytes 2097152 | tf_op jit(solution)/shard_map/all_to_all | solution.py:223
  131.3 1.1 copy-done.2
  132.4 10.4 %shard_map.102.refs_0_ = bf16[32,2,48,128]{3,2,1,0:T(8,128)(2,1)S(1)} custom-call(s32[1]{0:T(128)} %bitcast.tp_ref, bf16[32,2,48,256]{3,2,1,0:T(8,128)(2,1)S(1)} %all-to-all-done.refs_0_, bf16[32,2,48,256]{3,2,1,0:T(8,128)(2,1)} %collective-permute-done.refs_1_, bf16[32,2,48,256]{3,2,1,0:T(8,128)(2,1)} %collective-permute-done.1.refs_2_, ...), custom_call_target="tpu_custom_call" | custom-call | tf_op jit(solution)/shard_map/pallas_call | solution.py:185
  142.9 1.1 collective-permute-start.10
  144.0 2.8 %collective-permute-start.12 = (bf16[32,2,48,128]{3,2,1,0:T(8,128)(2,1)S(1)}, bf16[32,2,48,128]{3,2,1,0:T(8,128)(2,1)S(1)}, u32[]{:S(2)}, u32[]{:S(2)}) collective-permute-start(bf16[32,2,48,128]{3,2,1,0:T(8,128)(2,1)S(1)} %shard_map.102.refs_0_), channel_id=1, source_target_pairs={{0,6},{1,7},{2,0},{3,1},{4,2},{5,3},{6,4},{7,5},{8,14},{9,15},{10,... | collective-permute-start | bytes 2359304 | tf_op jit(solution)/shard_map/ppermute | solution.py:211
  146.7 17.5 %collective-permute-done.10.refs_2_ = bf16[32,2,48,128]{3,2,1,0:T(8,128)(2,1)S(1)} collective-permute-done((bf16[32,2,48,128]{3,2,1,0:T(8,128)(2,1)S(1)}, bf16[32,2,48,128]{3,2,1,0:T(8,128)(2,1)S(1)}, u32[]{:S(2)}, u32[]{:S(2)}) %collective-permute-start.10) | collective-permute-done | bytes 786464 | tf_op jit(solution)/shard_map/ppermute | solution.py:210
  164.4 3.3 %collective-permute-start.16 = (bf16[16,2,48,128]{3,2,1,0:T(8,128)(2,1)S(1)}, bf16[16,2,48,128]{3,2,1,0:T(8,128)(2,1)}, u32[]{:S(2)}, u32[]{:S(2)}) collective-permute-start(bf16[16,2,48,128]{3,2,1,0:T(8,128)(2,1)S(1)} %slice.27), channel_id=1, source_target_pairs={{0,6},{1,7},{2,0},{3,1},{4,2},{5,3},{6,4},{7,5},{8,14},{9,15},{10,... | collective-permute-start | bytes 1179656 | tf_op jit(solution)/shard_map/ppermute | solution.py:214
  168.2 7.6 %collective-permute-done.14.refs_6_ = bf16[16,2,48,128]{3,2,1,0:T(8,128)(2,1)S(1)} collective-permute-done((bf16[16,2,48,128]{3,2,1,0:T(8,128)(2,1)S(1)}, bf16[16,2,48,128]{3,2,1,0:T(8,128)(2,1)S(1)}, u32[]{:S(2)}, u32[]{:S(2)}) %collective-permute-start.14) | collective-permute-done | bytes 393248 | tf_op jit(solution)/shard_map/ppermute | solution.py:213
  176.3 1.3 collective-permute-done.15.refs_7_
  178.2 9.4 %shard_map.103 = bf16[32,2,48,256]{3,2,1,0:T(8,128)(2,1)} custom-call(s32[1]{0:T(128)} %bitcast.tp_ref, bf16[32,2,48,128]{3,2,1,0:T(8,128)(2,1)S(1)} %shard_map.102.refs_0_, bf16[32,2,48,128]{3,2,1,0:T(8,128)(2,1)S(1)} %collective-permute-done.9.refs_1_, bf16[32,2,48,128]{3,2,1,0:T(8,128)(2,1)S(1)} %collective-permute-done.10.refs_2_, ...), custom_call_target="tpu_custom_call" | custom-call | tf_op jit(solution)/shard_map/pallas_call | solution.py:185
  187.6 9.9 %all-to-all-start.3 = ((bf16[32,2,48,256]{3,2,1,0:T(8,128)(2,1)}), bf16[32,2,48,256]{3,2,1,0:T(8,128)(2,1)S(1)}, u32[]{:S(2)}, u32[]{:S(2)}) async-start(bf16[32,2,48,256]{3,2,1,0:T(8,128)(2,1)} %shard_map.103), calls=%async_computation.3 | async-start | bytes 3145728 | tf_op jit(solution)/shard_map/all_to_all | solution.py:223
  198.0 2.3 copy.17
  200.3 1.7 slice_bitcast_fusion
  202.0 1.0 copy.16
  203.0 1.0 copy.15
  204.0 33.1 %all-to-all-done.3 = bf16[32,2,48,256]{3,2,1,0:T(8,128)(2,1)S(1)} async-done(((bf16[32,2,48,256]{3,2,1,0:T(8,128)(2,1)}), bf16[32,2,48,256]{3,2,1,0:T(8,128)(2,1)S(1)}, u32[]{:S(2)}, u32[]{:S(2)}) %all-to-all-start.3) | async-done | bytes 1572896 | tf_op jit(solution)/shard_map/all_to_all | solution.py:223
  237.2 5.0 %combine.1 = bf16[768,256]{1,0:T(8,128)(2,1)} custom-call(s32[768,2]{1,0:T(8,128)S(1)} %bitcast.16, f32[768,2]{1,0:T(8,128)S(1)} %copy.14.affinity_ref, bf16[3072,256]{1,0:T(8,128)(2,1)S(1)} %bitcast.15), custom_call_target="tpu_custom_call" | custom-call | tf_op jit(solution)/shard_map/combine/pallas_call | solution.py:114
  (43 shorter events, 4.2 us)
Async XLA Ops:
  0.6 1.9 copy-start
  2.5 0.7 copy-start.3
  7.9 11.7 %copy-start.6 = (f32[64]{0:T(128)S(1)}, f32[64]{0:T(128)}, u32[]{:S(2)}) copy-start(f32[64]{0:T(128)} %param.10) | copy-start | bytes 772
  7.9 51.0 %all-to-all-start = ((bf16[32,2,48,256]{3,2,1,0:T(8,128)(2,1)}), bf16[32,2,48,256]{3,2,1,0:T(8,128)(2,1)S(1)}, u32[]{:S(2)}, u32[]{:S(2)}) async-start(bf16[32,2,48,256]{3,2,1,0:T(8,128)(2,1)} %bitcast.3), calls=%async_computation | async-start | bytes 3145728 | tf_op jit(solution)/shard_map/all_to_all | solution.py:223
  59.0 62.4 %all-to-all-start.1 = ((bf16[32,2,64,256]{3,2,1,0:T(8,128)(2,1)}), bf16[32,2,64,256]{3,2,1,0:T(8,128)(2,1)}, u32[]{:S(2)}, u32[]{:S(2)}) async-start(bf16[32,2,64,256]{3,2,1,0:T(8,128)(2,1)} %bitcast.18), calls=%async_computation.1 | async-start | bytes 4194304 | tf_op jit(solution)/shard_map/all_to_all | solution.py:223
  64.6 55.6 %copy-start.4 = (f32[64,32,256]{2,1,0:T(8,128)S(1)}, f32[64,32,256]{2,1,0:T(8,128)}, u32[]{:S(2)}) copy-start(f32[64,32,256]{2,1,0:T(8,128)} %param.13) | copy-start | bytes 6291460
  64.6 35.8 %collective-permute-start.1 = (bf16[32,2,48,256]{3,2,1,0:T(8,128)(2,1)S(1)}, bf16[32,2,48,256]{3,2,1,0:T(8,128)(2,1)}, u32[]{:S(2)}, u32[]{:S(2)}) collective-permute-start(bf16[32,2,48,256]{3,2,1,0:T(8,128)(2,1)S(1)} %all-to-all-done.refs_0_), channel_id=1, source_target_pairs={{0,2},{1,3},{2,4},{3,5},{4,6},{5,7},{6,0},{7,1},{8,10},{9,11},{10,... | collective-permute-start | bytes 4718600 | tf_op jit(solution)/shard_map/ppermute | solution.py:210
  66.2 35.8 %collective-permute-start.3 = (bf16[32,2,48,256]{3,2,1,0:T(8,128)(2,1)S(1)}, bf16[32,2,48,256]{3,2,1,0:T(8,128)(2,1)}, u32[]{:S(2)}, u32[]{:S(2)}) collective-permute-start(bf16[32,2,48,256]{3,2,1,0:T(8,128)(2,1)S(1)} %all-to-all-done.refs_0_), channel_id=1, source_target_pairs={{0,6},{1,7},{2,0},{3,1},{4,2},{5,3},{6,4},{7,5},{8,14},{9,15},{10,... | collective-permute-start | bytes 4718600 | tf_op jit(solution)/shard_map/ppermute | solution.py:211
  67.9 63.3 %collective-permute-start = (bf16[32,2,48,256]{3,2,1,0:T(8,128)(2,1)S(1)}, bf16[32,2,48,256]{3,2,1,0:T(8,128)(2,1)}, u32[]{:S(2)}, u32[]{:S(2)}) collective-permute-start(bf16[32,2,48,256]{3,2,1,0:T(8,128)(2,1)S(1)} %all-to-all-done.refs_0_), channel_id=1, source_target_pairs={{0,1},{1,0},{2,3},{3,2},{4,5},{5,4},{6,7},{7,6},{8,9},{9,8},{10,11... | collective-permute-start | bytes 4718600 | tf_op jit(solution)/shard_map/ppermute | solution.py:212
  101.6 18.0 %collective-permute-start.5 = (bf16[16,2,48,256]{3,2,1,0:T(8,128)(2,1)S(1)}, bf16[16,2,48,256]{3,2,1,0:T(8,128)(2,1)S(1)}, u32[]{:S(2)}, u32[]{:S(2)}) collective-permute-start(bf16[16,2,48,256]{3,2,1,0:T(8,128)(2,1)S(1)} %slice.24), channel_id=1, source_target_pairs={{0,2},{1,3},{2,4},{3,5},{4,6},{5,7},{6,0},{7,1},{8,10},{9,11},{10,... | collective-permute-start | bytes 2359304 | tf_op jit(solution)/shard_map/ppermute | solution.py:213
  103.2 17.0 %collective-permute-start.7 = (bf16[16,2,48,256]{3,2,1,0:T(8,128)(2,1)S(1)}, bf16[16,2,48,256]{3,2,1,0:T(8,128)(2,1)S(1)}, u32[]{:S(2)}, u32[]{:S(2)}) collective-permute-start(bf16[16,2,48,256]{3,2,1,0:T(8,128)(2,1)S(1)} %slice.25), channel_id=1, source_target_pairs={{0,6},{1,7},{2,0},{3,1},{4,2},{5,3},{6,4},{7,5},{8,14},{9,15},{10,... | collective-permute-start | bytes 2359304 | tf_op jit(solution)/shard_map/ppermute | solution.py:214
  106.2 25.1 %collective-permute-start.2 = (bf16[32,2,48,256]{3,2,1,0:T(8,128)(2,1)}, bf16[32,2,48,256]{3,2,1,0:T(8,128)(2,1)}, u32[]{:S(2)}, u32[]{:S(2)}) collective-permute-start(bf16[32,2,48,256]{3,2,1,0:T(8,128)(2,1)} %collective-permute-done.1.refs_2_), channel_id=1, source_target_pairs={{0,1},{1,0},{2,3},{3,2},{4,5},{5,4},{6,7},{7,6},{8,9},{9,8},{10,11... | collective-permute-start | bytes 4718600 | tf_op jit(solution)/shard_map/ppermute | solution.py:215
  106.2 25.1 %collective-permute-start.4 = (bf16[32,2,48,256]{3,2,1,0:T(8,128)(2,1)}, bf16[32,2,48,256]{3,2,1,0:T(8,128)(2,1)}, u32[]{:S(2)}, u32[]{:S(2)}) collective-permute-start(bf16[32,2,48,256]{3,2,1,0:T(8,128)(2,1)} %collective-permute-done.3.refs_4_), channel_id=1, source_target_pairs={{0,1},{1,0},{2,3},{3,2},{4,5},{5,4},{6,7},{7,6},{8,9},{9,8},{10,11... | collective-permute-start | bytes 4718600 | tf_op jit(solution)/shard_map/ppermute | solution.py:216
  119.6 11.6 %collective-permute-start.6 = (bf16[16,2,48,256]{3,2,1,0:T(8,128)(2,1)S(1)}, bf16[16,2,48,256]{3,2,1,0:T(8,128)(2,1)}, u32[]{:S(2)}, u32[]{:S(2)}) collective-permute-start(bf16[16,2,48,256]{3,2,1,0:T(8,128)(2,1)S(1)} %collective-permute-done.5.refs_6_), channel_id=1, source_target_pairs={{0,1},{1,0},{2,3},{3,2},{4,5},{5,4},{6,7},{7,6},{8,9},{9,8},{10,11... | collective-permute-start | bytes 2359304 | tf_op jit(solution)/shard_map/ppermute | solution.py:217
  120.1 1.2 copy-start.1
  120.1 11.1 %collective-permute-start.8 = (bf16[16,2,48,256]{3,2,1,0:T(8,128)(2,1)S(1)}, bf16[16,2,48,256]{3,2,1,0:T(8,128)(2,1)}, u32[]{:S(2)}, u32[]{:S(2)}) collective-permute-start(bf16[16,2,48,256]{3,2,1,0:T(8,128)(2,1)S(1)} %collective-permute-done.7.refs_8_), channel_id=1, source_target_pairs={{0,1},{1,0},{2,3},{3,2},{4,5},{5,4},{6,7},{7,6},{8,9},{9,8},{10,11... | collective-permute-start | bytes 2359304 | tf_op jit(solution)/shard_map/ppermute | solution.py:218
  121.4 54.9 %all-to-all-start.2 = ((bf16[32,2,32,256]{3,2,1,0:T(8,128)(2,1)}), bf16[32,2,32,256]{3,2,1,0:T(8,128)(2,1)}, u32[]{:S(2)}, u32[]{:S(2)}) async-start(bf16[32,2,32,256]{3,2,1,0:T(8,128)(2,1)} %bitcast.19), calls=%async_computation.2 | async-start | bytes 2097152 | tf_op jit(solution)/shard_map/all_to_all | solution.py:223
  131.3 1.1 copy-start.2
  142.9 21.3 %collective-permute-start.10 = (bf16[32,2,48,128]{3,2,1,0:T(8,128)(2,1)S(1)}, bf16[32,2,48,128]{3,2,1,0:T(8,128)(2,1)S(1)}, u32[]{:S(2)}, u32[]{:S(2)}) collective-permute-start(bf16[32,2,48,128]{3,2,1,0:T(8,128)(2,1)S(1)} %shard_map.102.refs_0_), channel_id=1, source_target_pairs={{0,2},{1,3},{2,4},{3,5},{4,6},{5,7},{6,0},{7,1},{8,10},{9,11},{10,... | collective-permute-start | bytes 2359304 | tf_op jit(solution)/shard_map/ppermute | solution.py:210
  144.0 20.4 %collective-permute-start.12 = (bf16[32,2,48,128]{3,2,1,0:T(8,128)(2,1)S(1)}, bf16[32,2,48,128]{3,2,1,0:T(8,128)(2,1)S(1)}, u32[]{:S(2)}, u32[]{:S(2)}) collective-permute-start(bf16[32,2,48,128]{3,2,1,0:T(8,128)(2,1)S(1)} %shard_map.102.refs_0_), channel_id=1, source_target_pairs={{0,6},{1,7},{2,0},{3,1},{4,2},{5,3},{6,4},{7,5},{8,14},{9,15},{10,... | collective-permute-start | bytes 2359304 | tf_op jit(solution)/shard_map/ppermute | solution.py:211
  146.7 29.6 %collective-permute-start.9 = (bf16[32,2,48,128]{3,2,1,0:T(8,128)(2,1)S(1)}, bf16[32,2,48,128]{3,2,1,0:T(8,128)(2,1)S(1)}, u32[]{:S(2)}, u32[]{:S(2)}) collective-permute-start(bf16[32,2,48,128]{3,2,1,0:T(8,128)(2,1)S(1)} %shard_map.102.refs_0_), channel_id=1, source_target_pairs={{0,1},{1,0},{2,3},{3,2},{4,5},{5,4},{6,7},{7,6},{8,9},{9,8},{10,11... | collective-permute-start | bytes 2359304 | tf_op jit(solution)/shard_map/ppermute | solution.py:212
  164.2 11.6 %collective-permute-start.14 = (bf16[16,2,48,128]{3,2,1,0:T(8,128)(2,1)S(1)}, bf16[16,2,48,128]{3,2,1,0:T(8,128)(2,1)S(1)}, u32[]{:S(2)}, u32[]{:S(2)}) collective-permute-start(bf16[16,2,48,128]{3,2,1,0:T(8,128)(2,1)S(1)} %slice.26), channel_id=1, source_target_pairs={{0,2},{1,3},{2,4},{3,5},{4,6},{5,7},{6,0},{7,1},{8,10},{9,11},{10,... | collective-permute-start | bytes 1179656 | tf_op jit(solution)/shard_map/ppermute | solution.py:213
  164.4 11.4 %collective-permute-start.16 = (bf16[16,2,48,128]{3,2,1,0:T(8,128)(2,1)S(1)}, bf16[16,2,48,128]{3,2,1,0:T(8,128)(2,1)}, u32[]{:S(2)}, u32[]{:S(2)}) collective-permute-start(bf16[16,2,48,128]{3,2,1,0:T(8,128)(2,1)S(1)} %slice.27), channel_id=1, source_target_pairs={{0,6},{1,7},{2,0},{3,1},{4,2},{5,3},{6,4},{7,5},{8,14},{9,15},{10,... | collective-permute-start | bytes 1179656 | tf_op jit(solution)/shard_map/ppermute | solution.py:214
  167.6 10.6 %collective-permute-start.11 = (bf16[32,2,48,128]{3,2,1,0:T(8,128)(2,1)S(1)}, bf16[32,2,48,128]{3,2,1,0:T(8,128)(2,1)}, u32[]{:S(2)}, u32[]{:S(2)}) collective-permute-start(bf16[32,2,48,128]{3,2,1,0:T(8,128)(2,1)S(1)} %collective-permute-done.10.refs_2_), channel_id=1, source_target_pairs={{0,1},{1,0},{2,3},{3,2},{4,5},{5,4},{6,7},{7,6},{8,9},{9,8},{10,11... | collective-permute-start | bytes 2359304 | tf_op jit(solution)/shard_map/ppermute | solution.py:215
  167.6 10.6 %collective-permute-start.13 = (bf16[32,2,48,128]{3,2,1,0:T(8,128)(2,1)S(1)}, bf16[32,2,48,128]{3,2,1,0:T(8,128)(2,1)}, u32[]{:S(2)}, u32[]{:S(2)}) collective-permute-start(bf16[32,2,48,128]{3,2,1,0:T(8,128)(2,1)S(1)} %collective-permute-done.12.refs_4_), channel_id=1, source_target_pairs={{0,1},{1,0},{2,3},{3,2},{4,5},{5,4},{6,7},{7,6},{8,9},{9,8},{10,11... | collective-permute-start | bytes 2359304 | tf_op jit(solution)/shard_map/ppermute | solution.py:216
  175.8 1.9 collective-permute-start.15
  175.8 2.4 collective-permute-start.17
  187.6 10.1 %copy-start.5 = (f32[768,2]{0,1:T(2,128)S(1)}, f32[768,2]{0,1:T(2,128)}, u32[]{:S(2)}) copy-start(f32[768,2]{0,1:T(2,128)} %param.9) | copy-start | bytes 18436
  187.6 49.6 %all-to-all-start.3 = ((bf16[32,2,48,256]{3,2,1,0:T(8,128)(2,1)}), bf16[32,2,48,256]{3,2,1,0:T(8,128)(2,1)S(1)}, u32[]{:S(2)}, u32[]{:S(2)}) async-start(bf16[32,2,48,256]{3,2,1,0:T(8,128)(2,1)} %shard_map.103), calls=%async_computation.3 | async-start | bytes 3145728 | tf_op jit(solution)/shard_map/all_to_all | solution.py:223

commit v2 on v0

v2 whole, which is shorter than its diff:
```python
import functools
import jax
import jax.numpy as jnp
from jax import lax
from jax.experimental import pallas as pl
from jax.experimental.pallas import tpu as pltpu
from jax.sharding import PartitionSpec as P

norm_eps = 1e-06
MIB = 1024 * 1024


def dispatch_kernel(cap, tp_ref, routes_ref, prompt_ref, out_ref, slots_ref, held, normed, key, choice, outbox, in_sem, out_sem):
    parts, rows, _ = held.shape
    experts, tokens = key.shape
    width = normed.shape[1]
    block = outbox.shape[1]
    loads = [
        pltpu.make_async_copy(prompt_ref.at[pl.ds(k * rows, rows)], held.at[k], in_sem.at[k])
        for k in range(parts)
    ]
    for load in loads:
        load.start()

    ids = routes_ref[...]
    expert = lax.broadcasted_iota(jnp.int32, (experts, tokens), 0)
    hit0 = ids[0:1, :] == expert
    hit1 = ids[1:2, :] == expert
    named = hit0 | hit1
    earlier = lax.broadcasted_iota(jnp.int32, (tokens, tokens), 0) < lax.broadcasted_iota(
        jnp.int32, (tokens, tokens), 1
    )
    count = jnp.dot(
        jnp.where(named, 1.0, 0.0).astype(jnp.bfloat16),
        jnp.where(earlier, 1.0, 0.0).astype(jnp.bfloat16),
        preferred_element_type=jnp.float32,
    )
    key[...] = jnp.where(named, count, -1.0).astype(jnp.int32)
    rank0 = jnp.sum(jnp.where(hit0, count, 0.0), axis=0, keepdims=True).astype(jnp.int32)
    rank1 = jnp.sum(jnp.where(hit1, count, 0.0), axis=0, keepdims=True).astype(jnp.int32)
    slots_ref[0:1, :] = ids[0:1, :] * cap + rank0
    slots_ref[1:2, :] = ids[1:2, :] * cap + rank1

    def fill(group, _):
        rank = lax.broadcasted_iota(jnp.int32, (cap, tokens), 0)
        first = pl.multiple_of(group * 8, 8)
        keys = key[pl.ds(first, 8), :]
        for k in range(8):
            choice[pl.ds(pl.multiple_of((first + k) * cap, cap), cap), :] = jnp.where(
                keys[k : k + 1, :] == rank, 1.0, 0.0
            ).astype(jnp.bfloat16)
        return 0

    lax.fori_loop(0, experts // 8, fill, 0)

    start = pl.multiple_of(tp_ref[0] * width, width)
    for k in range(parts):
        loads[k].wait()
        values = held[k].astype(jnp.float32)
        scale = lax.rsqrt(jnp.mean(values * values, axis=1, keepdims=True) + norm_eps)
        part = held[k, :, pl.ds(start, width)].astype(jnp.float32)
        normed[pl.ds(k * rows, rows), :] = (part * scale).astype(jnp.bfloat16)

    stores = []
    for k in range(outbox.shape[0]):
        outbox[k] = jnp.dot(
            choice[pl.ds(k * block, block), :], normed[...], preferred_element_type=jnp.float32
        ).astype(jnp.bfloat16)
        stores.append(
            pltpu.make_async_copy(outbox.at[k], out_ref.at[pl.ds(k * block, block)], out_sem.at[k])
        )
        stores[k].start()
    for store in stores:
        store.wait()


def dispatch(prompt, routes, tp_index, cap, experts, width):
    tokens, model_width = prompt.shape
    parts = 4
    rows, block = tokens // parts, experts * cap // parts
    return pl.pallas_call(
        functools.partial(dispatch_kernel, cap),
        in_specs=[
            pl.BlockSpec(memory_space=pltpu.SMEM),
            pl.BlockSpec(memory_space=pltpu.VMEM),
            pl.BlockSpec(memory_space=pltpu.HBM),
        ],
        out_specs=[
            pl.BlockSpec(memory_space=pltpu.HBM),
            pl.BlockSpec(memory_space=pltpu.VMEM),
        ],
        scratch_shapes=[
            pltpu.VMEM((parts, rows, model_width), jnp.bfloat16),
            pltpu.VMEM((tokens, width), jnp.bfloat16),
            pltpu.VMEM((experts, tokens), jnp.int32),
            pltpu.VMEM((experts * cap, tokens), jnp.bfloat16),
            pltpu.VMEM((parts, block, width), jnp.bfloat16),
            pltpu.SemaphoreType.DMA((parts,)),
            pltpu.SemaphoreType.DMA((parts,)),
        ],
        out_shape=[
            pltpu.HBM((experts * cap, width), jnp.bfloat16),
            jax.ShapeDtypeStruct((2, tokens), jnp.int32),
        ],
        compiler_params=pltpu.CompilerParams(vmem_limit_bytes=48 * MIB),
        name="dispatch",
    )(tp_index, routes.T, pltpu.with_memory_space_constraint(prompt, pltpu.HBM))


def combine_kernel(slots_ref, share_ref, rows_ref, out_ref):
    tokens = slots_ref.shape[1]
    block = rows_ref.shape[0] // 12
    share = share_ref[...]
    total = None
    for k in range(12):
        slot = lax.broadcasted_iota(jnp.int32, (block, tokens), 0) + k * block
        second = jnp.where(slots_ref[1:2, :] == slot, share[1:2, :], 0.0)
        weights = jnp.where(slots_ref[0:1, :] == slot, share[0:1, :], second).astype(jnp.bfloat16)
        product = lax.dot_general(
            weights,
            rows_ref[pl.ds(k * block, block), :],
            (((0,), (0,)), ((), ())),
            preferred_element_type=jnp.float32,
        )
        total = product if total is None else total + product
    out_ref[...] = total.astype(jnp.bfloat16)


def combine(slots, share, rows):
    whole = pl.BlockSpec(memory_space=pltpu.VMEM)
    return pl.pallas_call(
        combine_kernel,
        in_specs=[whole] * 3,
        out_specs=whole,
        out_shape=jax.ShapeDtypeStruct((slots.shape[1], rows.shape[1]), jnp.bfloat16),
        compiler_params=pltpu.CompilerParams(vmem_limit_bytes=48 * MIB),
        name="combine",
    )(slots, share, rows)


PLACES = ((0, 0), (0, 1), (3, 0), (3, 1), (1, 0), (1, 1), (2, 0), (2, 1))


def expert_matmul_kernel(gated, blocks, begin, out_begin, tp_ref, *refs):
    pieces, weight_ref, out_ref = refs[:8], refs[8], refs[-7]
    held, matrices, result, piece_sem, weight_sem, out_sem = refs[-6:]
    experts, count, cap, _ = held.shape
    width = pieces[0].shape[-1]
    group = matrices.shape[1] // 8
    index = tp_ref[0]

    loads = []
    for e in range(experts):
        for p in range(8):
            dx, swap = PLACES[p]
            source = (((index >> 1) + dx) & 3) * 2 + ((index & 1) ^ swap)
            first = begin if pieces[p].shape[0] > count else 0
            loads.append(
                pltpu.make_async_copy(
                    weight_ref.at[pl.ds(source * group, group), e],
                    matrices.at[e, pl.ds(p * group, group)],
                    weight_sem.at[e, p],
                )
            )
            loads.append(
                pltpu.make_async_copy(
                    pieces[p].at[pl.ds(first, count), e],
                    held.at[e, :, :, pl.ds(p * width, width)],
                    piece_sem.at[e, p],
                )
            )
    for load in loads:
        load.start()

    stores = []
    part = count // blocks
    for e in range(experts):
        for load in loads[16 * e : 16 * e + 16]:
            load.wait()
        right = matrices[e].reshape(8 * width, matrices.shape[-1])
        for b in range(blocks):
            span = pl.ds(b * part, part)
            left = held[e, span].reshape(part * cap, 8 * width)
            total = jnp.dot(left, right, preferred_element_type=jnp.float32)
            if gated:
                half = total.shape[1] // 2
                gate, up = total[:, :half], total[:, half:]
                total = gate / (1.0 + jnp.exp(-gate)) * up
            result[e, span] = total.astype(jnp.bfloat16).reshape((part,) + result.shape[2:])
        stores.append(
            pltpu.make_async_copy(
                result.at[e], out_ref.at[pl.ds(out_begin, count), e], out_sem.at[e]
            )
        )
        stores[e].start()
    for store in stores:
        store.wait()


def expert_matmul(pieces, weight, tp_index, half, gated, blocks, into):
    cap, width = pieces[0].shape[-2:]
    sources, experts = weight.shape[0], weight.shape[1]
    out_width = weight.shape[-1] // 2 if gated else weight.shape[-1]
    count = sources // 2
    anywhere = pl.BlockSpec(memory_space=pl.ANY)
    operands = [*pieces, weight]
    aliases = {}
    if into is not None:
        operands.append(into)
        aliases = {len(operands): 0}
    out_shape = pltpu.HBM((count if gated else sources, experts, cap, out_width), jnp.bfloat16)
    operands = [pltpu.with_memory_space_constraint(array, pltpu.HBM) for array in operands]
    return pl.pallas_call(
        functools.partial(
            expert_matmul_kernel, gated, blocks, half * count, 0 if gated else half * count
        ),
        in_specs=[pl.BlockSpec(memory_space=pltpu.SMEM)] + [anywhere] * len(operands),
        out_specs=pl.BlockSpec(memory_space=pltpu.HBM),
        out_shape=out_shape,
        scratch_shapes=[
            pltpu.VMEM((experts, count, cap, 8 * width), jnp.bfloat16),
            pltpu.VMEM((experts, sources) + weight.shape[2:], jnp.bfloat16),
            pltpu.VMEM((experts, count, cap, out_width), jnp.bfloat16),
            pltpu.SemaphoreType.DMA((experts, 8)),
            pltpu.SemaphoreType.DMA((experts, 8)),
            pltpu.SemaphoreType.DMA((experts,)),
        ],
        input_output_aliases=aliases,
        compiler_params=pltpu.CompilerParams(vmem_limit_bytes=48 * MIB),
    )(tp_index, *operands)


def tp_move(dx, swap):
    return [(2 * x + c, 2 * ((x + dx) % 4) + (c ^ swap)) for x in range(4) for c in range(2)]


def move(array, dx, swap):
    return lax.ppermute(array, "tp", tp_move(dx, swap))


def spread_tokens(own):
    half = own.shape[0] // 2
    first, second = own[:half], own[half:]
    right_first = move(first, 1, 0)
    left_second = move(second, 3, 0)
    right_second = move(second, 1, 0)
    left_first = move(first, 3, 0)
    own_other = move(own, 0, 1)
    far_first = move(right_first, 1, 0)
    far_second = move(left_second, 3, 0)

    def both(piece):
        return piece, move(piece, 0, 1)

    return (
        (own, own_other)
        + both(right_first)
        + both(left_first)
        + both(far_first),
        (own, own_other)
        + both(right_second)
        + both(left_second)
        + both(far_second),
    )


def spread_hidden(own, half):
    right = move(own, 1, 0)
    left = move(own, 3, 0)
    far = move(right, 1, 0) if half == 0 else move(left, 3, 0)
    own_other = move(own, 0, 1)
    right_other = move(right, 0, 1)
    left_other = move(left, 0, 1)
    far_other = move(far, 0, 1)
    return own, own_other, right, right_other, left, left_other, far, far_other


def exchange(array):
    return lax.all_to_all(array, "fs", split_axis=0, concat_axis=0, tiled=True)


def layer(prompt, routes, affinity, norm_gain, gate_master, up_master, down_master):
    fs_count, tp_count = lax.axis_size("fs"), lax.axis_size("tp")
    experts, gain_rows, hidden_width = gate_master.shape
    here = experts // fs_count
    token_count, top_count = routes.shape
    capacity = 2 * token_count * top_count // experts
    width = prompt.shape[1] // tp_count
    tp_index = lax.axis_index("tp").astype(jnp.int32)
    tp_index = tp_index.reshape(1)

    outbox, slots = dispatch(prompt, routes, tp_index, capacity, experts, width)
    received = exchange(outbox.reshape(fs_count, here, capacity, width))

    gain = norm_gain[None, :, None]
    gate_up = jnp.concatenate(
        [(gate_master * gain).astype(jnp.bfloat16), (up_master * gain).astype(jnp.bfloat16)], axis=2
    ).reshape(fs_count, here, gain_rows, 2 * hidden_width)
    pieces = spread_tokens(received)
    swapped = [piece for half in pieces for piece in half[1::2]]
    affinity = lax.optimization_barrier((affinity, *swapped))[0].T
    share = affinity / jnp.sum(affinity, axis=0, keepdims=True)
    down = down_master.astype(jnp.bfloat16).reshape((fs_count, here) + down_master.shape[1:])
    gate_up_new = exchange(gate_up)
    down_new = exchange(down)
    hidden = [
        spread_hidden(expert_matmul(pieces[half], gate_up_new, tp_index, half, True, 2, None), half)
        for half in range(2)
    ]
    expert_out = None
    for half in range(2):
        expert_out = expert_matmul(hidden[half], down_new, tp_index, half, False, 2, expert_out)
    returned = exchange(expert_out)
    mixed = combine(slots, share, returned.reshape(experts * capacity, width))

    def rows_first(array):
        return array.transpose(1, 0, 2, 3).reshape(here, -1, array.shape[-1])

    return (
        mixed,
        rows_first(gate_up_new[..., :hidden_width]),
        rows_first(gate_up_new[..., hidden_width:]),
        rows_first(down_new),
    )


def solution(mesh):
    in_specs = (
        P("fs", None),
        P("fs", None),
        P("fs", None),
        P("fs"),
        P(None, "fs", "tp"),
        P(None, "fs", "tp"),
        P(None, "fs", "tp"),
    )
    out_specs = (P("fs", "tp"), P("fs", None, "tp"), P("fs", None, "tp"), P("fs", None, "tp"))
    return jax.shard_map(layer, mesh=mesh, in_specs=in_specs, out_specs=out_specs, check_vma=False)
```

time: 311 us -> 223 us (0.72)
  blocking collectives: 144 us -> 0 us
  waiting for transfers between devices: 60.8 us -> 129 us
  starting transfers between devices: 10.4 us -> 52 us
  other arithmetic: 33.8 us -> 5.69 us
  Pallas kernels: 0 us -> 26 us
  local copies, waits for them, and re-layouts: 29.9 us -> 9.35 us
  matrix products: 17 us -> 0 us
  between operations: 14.4 us -> 0.97 us
    all_to_all x3 -> x0, blocking collectives: 144 us -> none  [the longest x1 55.1 us: side_by_side(): lax.all_to_all(both, axis, split_axis=split_dim, concat_axis=concat_dim,...]
    ppermute x0 -> x27, waiting for transfers between devices: none -> 52.4 us  [move(): return lax.ppermute(array, 'tp', tp_move(dx, swap))]
    all_to_all x1 -> x4, waiting for transfers between devices: 39.5 us -> 76.2 us  [exchange(): return lax.all_to_all(array, 'fs', split_axis=0, concat_axis=0, tiled=True)]
    pallas_call x0 -> x6, Pallas kernels: none -> 26 us  [the longest x4 18.6 us: expert_matmul(): pl.pallas_call(functools.partial(expert_matmul_kernel, gated, blocks, hal...]
    all_to_all x1 -> x4, starting transfers between devices: 10.3 us -> 33.3 us  [exchange(): return lax.all_to_all(array, 'fs', split_axis=0, concat_axis=0, tiled=True)]
    all_gather x2 -> x0, waiting for transfers between devices: 21.3 us -> none  [the longest x1 11.9 us: per_device(): shard_piece = lax.all_gather(received, 'tp', axis=2, tiled=True)]
    ppermute x0 -> x27, starting transfers between devices: none -> 18.6 us  [move(): return lax.ppermute(array, 'tp', tp_move(dx, swap))]
    another operation x3 -> x0, other arithmetic: 18.4 us -> none
  transfers between devices with their start and end apart: 3 -> 31, of which waited for: 3 -> 13; matrix products, arithmetic and copies ran while one was open for 1% -> 5% of each run, Pallas kernels for 0% -> 7%
where the time goes in v2:
time: 223 us
  waiting for transfers between devices  129 us (58%)
  starting transfers between devices  52 us (23%)
  Pallas kernels  26 us (12%)
  local copies, waits for them, and re-layouts  9.35 us (4%)
  other arithmetic  5.69 us (3%)
    all_to_all x4, waiting for transfers between devices, exchange(): return lax.all_to_all(array, 'fs', split_axis=0, concat_axis=0, tiled=True)  76.2 us
    ppermute x27, waiting for transfers between devices, move(): return lax.ppermute(array, 'tp', tp_move(dx, swap))  52.4 us
    all_to_all x4, starting transfers between devices, exchange(): return lax.all_to_all(array, 'fs', split_axis=0, concat_axis=0, tiled=True)  33.3 us
    ppermute x27, starting transfers between devices, move(): return lax.ppermute(array, 'tp', tp_move(dx, swap))  18.6 us
    pallas_call x4, Pallas kernels, expert_matmul(): pl.pallas_call(functools.partial(expert_matmul_kernel, gated, blocks, hal...  18.6 us
    transpose x4, local copies, waits for them, and re-layouts, rows_first(): return array.transpose(1, 0, 2, 3).reshape(here, -1, array.shape[-1])  4.84 us
    pallas_call x1, Pallas kernels, dispatch(): pl.pallas_call(functools.partial(dispatch_kernel, cap), in_specs=[pl.Bloc...  4.7 us
  transfers between devices with their start and end apart: 31, of which 13 were waited for; matrix products, arithmetic and copies ran while one was open for 5% of the time, Pallas kernels for 7%

profile of v2, /device:TPU:16, one launch (start us, length us, event | category | flops | bytes accessed | tf_op | source)
XLA Modules:
  0.0 222.6 jit_solution(9927095636624896176)
XLA Ops:
  1.3 4.7 %dispatch.1 = (bf16[3072,256]{1,0:T(8,128)(2,1)}, s32[2,768]{1,0:T(2,128)S(1)}) custom-call(s32[1]{0:T(128)} %bitcast.tp_ref, s32[2,768]{1,0:T(2,128)S(1)} %bitcast.17, bf16[768,2048]{1,0:T(8,128)(2,1)} %prompt_ref.1), custom_call_target="tpu_custom_call" | custom-call | tf_op jit(solution)/shard_map/dispatch/pallas_call | solution.py:81
  6.0 11.6 %all-to-all-start = ((bf16[32,2,48,256]{3,2,1,0:T(8,128)(2,1)}), bf16[32,2,48,256]{3,2,1,0:T(8,128)(2,1)S(1)}, u32[]{:S(2)}, u32[]{:S(2)}) async-start(bf16[32,2,48,256]{3,2,1,0:T(8,128)(2,1)} %bitcast.21), calls=%async_computation | async-start | bytes 3145728 | tf_op jit(solution)/shard_map/all_to_all | solution.py:279
  17.7 2.9 %multiply_convert_fusion.1 = (bf16[64,64,128]{2,1,0:T(8,128)(2,1)S(1)}, bf16[64,64,128]{2,1,0:T(8,128)(2,1)S(1)}) fusion(f32[64,64,128]{2,1,0:T(8,128)} %param.11, f32[64]{0:T(128)S(1)} %copy-done.18, f32[64,64,128]{2,1,0:T(8,128)} %param.12), kind=kLoop, calls=%fused_computation.2 | loop fusion | flops 2097152 | bytes 6291712 | tf_op jit(solution)/shard_map/convert_element_type | solution.py:297
  20.5 1.7 pad_maximum_fusion
  22.2 34.7 %all-to-all-done.refs_0_ = bf16[32,2,48,256]{3,2,1,0:T(8,128)(2,1)S(1)} async-done(((bf16[32,2,48,256]{3,2,1,0:T(8,128)(2,1)}), bf16[32,2,48,256]{3,2,1,0:T(8,128)(2,1)S(1)}, u32[]{:S(2)}, u32[]{:S(2)}) %all-to-all-start) | async-done | bytes 1572896 | tf_op jit(solution)/shard_map/all_to_all | solution.py:279
  56.9 5.6 %all-to-all-start.1 = ((bf16[32,2,64,256]{3,2,1,0:T(8,128)(2,1)}), bf16[32,2,64,256]{3,2,1,0:T(8,128)(2,1)}, u32[]{:S(2)}, u32[]{:S(2)}) async-start(bf16[32,2,64,256]{3,2,1,0:T(8,128)(2,1)} %bitcast.19), calls=%async_computation.1 | async-start | bytes 4194304 | tf_op jit(solution)/shard_map/all_to_all | solution.py:279
  62.7 1.6 collective-permute-start.1
  64.3 1.7 collective-permute-start.3
  66.0 1.5 collective-permute-start.9
  68.0 16.5 %collective-permute-done.1.refs_2_ = bf16[16,2,48,256]{3,2,1,0:T(8,128)(2,1)} collective-permute-done((bf16[16,2,48,256]{3,2,1,0:T(8,128)(2,1)S(1)}, bf16[16,2,48,256]{3,2,1,0:T(8,128)(2,1)}, u32[]{:S(2)}, u32[]{:S(2)}) %collective-permute-start.1) | collective-permute-done | bytes 786464 | tf_op jit(solution)/shard_map/ppermute | solution.py:238
  84.8 13.6 %collective-permute-done.9.refs_4_ = bf16[16,2,48,256]{3,2,1,0:T(8,128)(2,1)S(1)} collective-permute-done((bf16[16,2,48,256]{3,2,1,0:T(8,128)(2,1)S(1)}, bf16[16,2,48,256]{3,2,1,0:T(8,128)(2,1)S(1)}, u32[]{:S(2)}, u32[]{:S(2)}) %collective-permute-start.9) | collective-permute-done | bytes 786464 | tf_op jit(solution)/shard_map/ppermute | solution.py:238
  98.4 2.8 %collective-permute-done.7.refs_2_ = bf16[16,2,48,256]{3,2,1,0:T(8,128)(2,1)S(1)} collective-permute-done((bf16[16,2,48,256]{3,2,1,0:T(8,128)(2,1)S(1)}, bf16[16,2,48,256]{3,2,1,0:T(8,128)(2,1)S(1)}, u32[]{:S(2)}, u32[]{:S(2)}) %collective-permute-start.7) | collective-permute-done | bytes 786464 | tf_op jit(solution)/shard_map/ppermute | solution.py:238
  102.1 1.5 collective-permute-start.11
  103.7 1.1 convert_element_type.11
  104.8 6.6 %all-to-all-done.1.refs_8_ = bf16[32,2,64,256]{3,2,1,0:T(8,128)(2,1)} async-done(((bf16[32,2,64,256]{3,2,1,0:T(8,128)(2,1)}), bf16[32,2,64,256]{3,2,1,0:T(8,128)(2,1)}, u32[]{:S(2)}, u32[]{:S(2)}) %all-to-all-start.1) | async-done | bytes 2097184 | tf_op jit(solution)/shard_map/all_to_all | solution.py:279
  111.4 6.2 %all-to-all-start.2 = ((bf16[32,2,32,256]{3,2,1,0:T(8,128)(2,1)}), bf16[32,2,32,256]{3,2,1,0:T(8,128)(2,1)S(1)}, u32[]{:S(2)}, u32[]{:S(2)}) async-start(bf16[32,2,32,256]{3,2,1,0:T(8,128)(2,1)} %bitcast.20), calls=%async_computation.2 | async-start | bytes 2097152 | tf_op jit(solution)/shard_map/all_to_all | solution.py:279
  118.5 1.2 collective-permute-done.11.refs_6_
  121.1 5.4 %shard_map.103.refs_0_ = bf16[16,2,48,128]{3,2,1,0:T(8,128)(2,1)} custom-call(s32[1]{0:T(128)} %bitcast.tp_ref, bf16[32,2,48,256]{3,2,1,0:T(8,128)(2,1)} %copy-done.1, bf16[32,2,48,256]{3,2,1,0:T(8,128)(2,1)} %collective-permute-done.refs_1_, bf16[16,2,48,256]{3,2,1,0:T(8,128)(2,1)} %collective-permute-done.1.refs_2_, ...), custom_call_target="tpu_custom_call" | custom-call | tf_op jit(solution)/shard_map/pallas_call | solution.py:213
  126.5 1.6 collective-permute-start.21
  128.0 2.0 collective-permute-start.23
  132.0 5.4 %shard_map.102.refs_0_ = bf16[16,2,48,128]{3,2,1,0:T(8,128)(2,1)} custom-call(s32[1]{0:T(128)} %bitcast.tp_ref, bf16[32,2,48,256]{3,2,1,0:T(8,128)(2,1)} %copy-done.1, bf16[32,2,48,256]{3,2,1,0:T(8,128)(2,1)} %collective-permute-done.refs_1_, bf16[16,2,48,256]{3,2,1,0:T(8,128)(2,1)} %copy-done.6, bf16[16,2,48,256]{3,2,1,0:T(8,128)(2,1)} %copy-done.8, ...), custom_call_target="tpu_custom_call" | custom-call | tf_op jit(solution)/shard_map/pallas_call | solution.py:213
  137.4 2.0 collective-permute-start.16
  140.5 8.6 %collective-permute-done.16.refs_4_ = bf16[16,2,48,128]{3,2,1,0:T(8,128)(2,1)} collective-permute-done((bf16[16,2,48,128]{3,2,1,0:T(8,128)(2,1)}, bf16[16,2,48,128]{3,2,1,0:T(8,128)(2,1)}, u32[]{:S(2)}, u32[]{:S(2)}) %collective-permute-start.16) | collective-permute-done | bytes 393248 | tf_op jit(solution)/shard_map/ppermute | solution.py:238
  149.1 3.1 %collective-permute-start.18 = (bf16[16,2,48,128]{3,2,1,0:T(8,128)(2,1)}, bf16[16,2,48,128]{3,2,1,0:T(8,128)(2,1)}, u32[]{:S(2)}, u32[]{:S(2)}) collective-permute-start(bf16[16,2,48,128]{3,2,1,0:T(8,128)(2,1)} %collective-permute-done.16.refs_4_), channel_id=1, source_target_pairs={{0,6},{1,7},{2,0},{3,1},{4,2},{5,3},{6,4},{7,5},{8,14},{9,15},{10,... | collective-permute-start | bytes 1179656 | tf_op jit(solution)/shard_map/ppermute | solution.py:238
  152.9 7.3 %collective-permute-done.25.refs_6_ = bf16[16,2,48,128]{3,2,1,0:T(8,128)(2,1)S(1)} collective-permute-done((bf16[16,2,48,128]{3,2,1,0:T(8,128)(2,1)S(1)}, bf16[16,2,48,128]{3,2,1,0:T(8,128)(2,1)S(1)}, u32[]{:S(2)}, u32[]{:S(2)}) %collective-permute-start.25) | collective-permute-done | bytes 393248 | tf_op jit(solution)/shard_map/ppermute | solution.py:238
  162.3 3.9 %shard_map.104.refs_9_ = bf16[32,2,48,256]{3,2,1,0:T(8,128)(2,1)} custom-call(s32[1]{0:T(128)} %bitcast.tp_ref, bf16[16,2,48,128]{3,2,1,0:T(8,128)(2,1)} %shard_map.103.refs_0_, bf16[16,2,48,128]{3,2,1,0:T(8,128)(2,1)} %copy-done.13, bf16[16,2,48,128]{3,2,1,0:T(8,128)(2,1)} %copy-done.11, bf16[16,2,48,128]{3,2,1,0:T(8,128)(2,1)} %copy-done.15, ...), custom_call_target="tpu_custom_call" | custom-call | tf_op jit(solution)/shard_map/pallas_call | solution.py:213
  166.2 4.0 %shard_map.105 = bf16[32,2,48,256]{3,2,1,0:T(8,128)(2,1)} custom-call(s32[1]{0:T(128)} %bitcast.tp_ref, bf16[16,2,48,128]{3,2,1,0:T(8,128)(2,1)} %shard_map.102.refs_0_, bf16[16,2,48,128]{3,2,1,0:T(8,128)(2,1)} %collective-permute-done.13.refs_1_, bf16[16,2,48,128]{3,2,1,0:T(8,128)(2,1)} %collective-permute-done.14.refs_2_, ...), custom_call_target="tpu_custom_call", output_to_operand_aliasing={{}: (10, {})} | custom-call | tf_op jit(solution)/shard_map/pallas_call | solution.py:213
  170.2 9.9 %all-to-all-start.3 = ((bf16[32,2,48,256]{3,2,1,0:T(8,128)(2,1)}), bf16[32,2,48,256]{3,2,1,0:T(8,128)(2,1)S(1)}, u32[]{:S(2)}, u32[]{:S(2)}) async-start(bf16[32,2,48,256]{3,2,1,0:T(8,128)(2,1)} %shard_map.105), calls=%async_computation.3 | async-start | bytes 3145728 | tf_op jit(solution)/shard_map/all_to_all | solution.py:279
  180.1 1.1 copy.14
  181.2 1.7 slice_bitcast_fusion
  185.0 34.9 %all-to-all-done.3 = bf16[32,2,48,256]{3,2,1,0:T(8,128)(2,1)S(1)} async-done(((bf16[32,2,48,256]{3,2,1,0:T(8,128)(2,1)}), bf16[32,2,48,256]{3,2,1,0:T(8,128)(2,1)S(1)}, u32[]{:S(2)}, u32[]{:S(2)}) %all-to-all-start.3) | async-done | bytes 1572896 | tf_op jit(solution)/shard_map/all_to_all | solution.py:279
  219.9 2.7 %combine.1 = bf16[768,256]{1,0:T(8,128)(2,1)} custom-call(s32[2,768]{1,0:T(2,128)S(1)} %get-tuple-element.7.slots_ref, f32[2,768]{1,0:T(2,128)S(1)} %divide_bitcast_fusion.share_ref, bf16[3072,256]{1,0:T(8,128)(2,1)S(1)} %bitcast.16), custom_call_target="tpu_custom_call" | custom-call | tf_op jit(solution)/shard_map/combine/pallas_call | solution.py:131
  (84 shorter events, 12.5 us)
Async XLA Ops:
  6.0 50.9 %all-to-all-start = ((bf16[32,2,48,256]{3,2,1,0:T(8,128)(2,1)}), bf16[32,2,48,256]{3,2,1,0:T(8,128)(2,1)S(1)}, u32[]{:S(2)}, u32[]{:S(2)}) async-start(bf16[32,2,48,256]{3,2,1,0:T(8,128)(2,1)} %bitcast.21), calls=%async_computation | async-start | bytes 3145728 | tf_op jit(solution)/shard_map/all_to_all | solution.py:279
  56.9 54.4 %all-to-all-start.1 = ((bf16[32,2,64,256]{3,2,1,0:T(8,128)(2,1)}), bf16[32,2,64,256]{3,2,1,0:T(8,128)(2,1)}, u32[]{:S(2)}, u32[]{:S(2)}) async-start(bf16[32,2,64,256]{3,2,1,0:T(8,128)(2,1)} %bitcast.19), calls=%async_computation.1 | async-start | bytes 4194304 | tf_op jit(solution)/shard_map/all_to_all | solution.py:279
  62.6 41.1 %copy-start.4 = (f32[64,32,256]{2,1,0:T(8,128)S(1)}, f32[64,32,256]{2,1,0:T(8,128)}, u32[]{:S(2)}) copy-start(f32[64,32,256]{2,1,0:T(8,128)} %param.13) | copy-start | bytes 6291460
  62.7 21.8 %collective-permute-start.1 = (bf16[16,2,48,256]{3,2,1,0:T(8,128)(2,1)S(1)}, bf16[16,2,48,256]{3,2,1,0:T(8,128)(2,1)}, u32[]{:S(2)}, u32[]{:S(2)}) collective-permute-start(bf16[16,2,48,256]{3,2,1,0:T(8,128)(2,1)S(1)} %get-tuple-element.13), channel_id=1, source_target_pairs={{0,2},{1,3},{2,4},{3,5},{4,6},{5,7},{6,0},{7,1},{8,10},{9,11},{10,... | collective-permute-start | bytes 2359304 | tf_op jit(solution)/shard_map/ppermute | solution.py:238
  64.3 20.5 %collective-permute-start.3 = (bf16[16,2,48,256]{3,2,1,0:T(8,128)(2,1)S(1)}, bf16[16,2,48,256]{3,2,1,0:T(8,128)(2,1)}, u32[]{:S(2)}, u32[]{:S(2)}) collective-permute-start(bf16[16,2,48,256]{3,2,1,0:T(8,128)(2,1)S(1)} %get-tuple-element.13), channel_id=1, source_target_pairs={{0,6},{1,7},{2,0},{3,1},{4,2},{5,3},{6,4},{7,5},{8,14},{9,15},{10,... | collective-permute-start | bytes 2359304 | tf_op jit(solution)/shard_map/ppermute | solution.py:238
  66.0 32.4 %collective-permute-start.9 = (bf16[16,2,48,256]{3,2,1,0:T(8,128)(2,1)S(1)}, bf16[16,2,48,256]{3,2,1,0:T(8,128)(2,1)S(1)}, u32[]{:S(2)}, u32[]{:S(2)}) collective-permute-start(bf16[16,2,48,256]{3,2,1,0:T(8,128)(2,1)S(1)} %get-tuple-element.12), channel_id=1, source_target_pairs={{0,6},{1,7},{2,0},{3,1},{4,2},{5,3},{6,4},{7,5},{8,14},{9,15},{10,... | collective-permute-start | bytes 2359304 | tf_op jit(solution)/shard_map/ppermute | solution.py:238
  67.6 33.7 %collective-permute-start.7 = (bf16[16,2,48,256]{3,2,1,0:T(8,128)(2,1)S(1)}, bf16[16,2,48,256]{3,2,1,0:T(8,128)(2,1)S(1)}, u32[]{:S(2)}, u32[]{:S(2)}) collective-permute-start(bf16[16,2,48,256]{3,2,1,0:T(8,128)(2,1)S(1)} %get-tuple-element.12), channel_id=1, source_target_pairs={{0,2},{1,3},{2,4},{3,5},{4,6},{5,7},{6,0},{7,1},{8,10},{9,11},{10,... | collective-permute-start | bytes 2359304 | tf_op jit(solution)/shard_map/ppermute | solution.py:238
  68.0 51.7 %collective-permute-start = (bf16[32,2,48,256]{3,2,1,0:T(8,128)(2,1)S(1)}, bf16[32,2,48,256]{3,2,1,0:T(8,128)(2,1)}, u32[]{:S(2)}, u32[]{:S(2)}) collective-permute-start(bf16[32,2,48,256]{3,2,1,0:T(8,128)(2,1)S(1)} %all-to-all-done.refs_0_), channel_id=1, source_target_pairs={{0,1},{1,0},{2,3},{3,2},{4,5},{5,4},{6,7},{7,6},{8,9},{9,8},{10,11... | collective-permute-start | bytes 4718600 | tf_op jit(solution)/shard_map/ppermute | solution.py:238
  84.5 33.1 %collective-permute-start.5 = (bf16[16,2,48,256]{3,2,1,0:T(8,128)(2,1)}, bf16[16,2,48,256]{3,2,1,0:T(8,128)(2,1)}, u32[]{:S(2)}, u32[]{:S(2)}) collective-permute-start(bf16[16,2,48,256]{3,2,1,0:T(8,128)(2,1)} %collective-permute-done.1.refs_2_), channel_id=1, source_target_pairs={{0,2},{1,3},{2,4},{3,5},{4,6},{5,7},{6,0},{7,1},{8,10},{9,11},{10,... | collective-permute-start | bytes 2359304 | tf_op jit(solution)/shard_map/ppermute | solution.py:238
  84.8 32.9 %collective-permute-start.2 = (bf16[16,2,48,256]{3,2,1,0:T(8,128)(2,1)}, bf16[16,2,48,256]{3,2,1,0:T(8,128)(2,1)}, u32[]{:S(2)}, u32[]{:S(2)}) collective-permute-start(bf16[16,2,48,256]{3,2,1,0:T(8,128)(2,1)} %collective-permute-done.1.refs_2_), channel_id=1, source_target_pairs={{0,1},{1,0},{2,3},{3,2},{4,5},{5,4},{6,7},{7,6},{8,9},{9,8},{10,11... | collective-permute-start | bytes 2359304 | tf_op jit(solution)/shard_map/ppermute | solution.py:238
  98.4 19.8 %collective-permute-start.4 = (bf16[16,2,48,256]{3,2,1,0:T(8,128)(2,1)}, bf16[16,2,48,256]{3,2,1,0:T(8,128)(2,1)}, u32[]{:S(2)}, u32[]{:S(2)}) collective-permute-start(bf16[16,2,48,256]{3,2,1,0:T(8,128)(2,1)} %collective-permute-done.3.refs_4_), channel_id=1, source_target_pairs={{0,1},{1,0},{2,3},{3,2},{4,5},{5,4},{6,7},{7,6},{8,9},{9,8},{10,11... | collective-permute-start | bytes 2359304 | tf_op jit(solution)/shard_map/ppermute | solution.py:238
  102.1 17.6 %collective-permute-start.11 = (bf16[16,2,48,256]{3,2,1,0:T(8,128)(2,1)S(1)}, bf16[16,2,48,256]{3,2,1,0:T(8,128)(2,1)}, u32[]{:S(2)}, u32[]{:S(2)}) collective-permute-start(bf16[16,2,48,256]{3,2,1,0:T(8,128)(2,1)S(1)} %collective-permute-done.9.refs_4_), channel_id=1, source_target_pairs={{0,6},{1,7},{2,0},{3,1},{4,2},{5,3},{6,4},{7,5},{8,14},{9,15},{10,... | collective-permute-start | bytes 2359304 | tf_op jit(solution)/shard_map/ppermute | solution.py:238
  111.4 49.9 %all-to-all-start.2 = ((bf16[32,2,32,256]{3,2,1,0:T(8,128)(2,1)}), bf16[32,2,32,256]{3,2,1,0:T(8,128)(2,1)S(1)}, u32[]{:S(2)}, u32[]{:S(2)}) async-start(bf16[32,2,32,256]{3,2,1,0:T(8,128)(2,1)} %bitcast.20), calls=%async_computation.2 | async-start | bytes 2097152 | tf_op jit(solution)/shard_map/all_to_all | solution.py:279
  117.6 2.6 %collective-permute-start.6 = (bf16[16,2,48,256]{3,2,1,0:T(8,128)(2,1)}, bf16[16,2,48,256]{3,2,1,0:T(8,128)(2,1)S(1)}, u32[]{:S(2)}, u32[]{:S(2)}) collective-permute-start(bf16[16,2,48,256]{3,2,1,0:T(8,128)(2,1)} %collective-permute-done.5.refs_6_), channel_id=1, source_target_pairs={{0,1},{1,0},{2,3},{3,2},{4,5},{5,4},{6,7},{7,6},{8,9},{9,8},{10,11... | collective-permute-start | bytes 2359304 | tf_op jit(solution)/shard_map/ppermute | solution.py:238
  117.7 12.3 %collective-permute-start.10 = (bf16[16,2,48,256]{3,2,1,0:T(8,128)(2,1)S(1)}, bf16[16,2,48,256]{3,2,1,0:T(8,128)(2,1)S(1)}, u32[]{:S(2)}, u32[]{:S(2)}) collective-permute-start(bf16[16,2,48,256]{3,2,1,0:T(8,128)(2,1)S(1)} %collective-permute-done.9.refs_4_), channel_id=1, source_target_pairs={{0,1},{1,0},{2,3},{3,2},{4,5},{5,4},{6,7},{7,6},{8,9},{9,8},{10,11... | collective-permute-start | bytes 2359304 | tf_op jit(solution)/shard_map/ppermute | solution.py:238
  118.2 12.0 %collective-permute-start.8 = (bf16[16,2,48,256]{3,2,1,0:T(8,128)(2,1)}, bf16[16,2,48,256]{3,2,1,0:T(8,128)(2,1)S(1)}, u32[]{:S(2)}, u32[]{:S(2)}) collective-permute-start(bf16[16,2,48,256]{3,2,1,0:T(8,128)(2,1)} %copy-done.6), channel_id=1, source_target_pairs={{0,1},{1,0},{2,3},{3,2},{4,5},{5,4},{6,7},{7,6},{8,9},{9,8},{10,11... | collective-permute-start | bytes 2359304 | tf_op jit(solution)/shard_map/ppermute | solution.py:238
  119.7 10.5 %collective-permute-start.12 = (bf16[16,2,48,256]{3,2,1,0:T(8,128)(2,1)}, bf16[16,2,48,256]{3,2,1,0:T(8,128)(2,1)S(1)}, u32[]{:S(2)}, u32[]{:S(2)}) collective-permute-start(bf16[16,2,48,256]{3,2,1,0:T(8,128)(2,1)} %collective-permute-done.11.refs_6_), channel_id=1, source_target_pairs={{0,1},{1,0},{2,3},{3,2},{4,5},{5,4},{6,7},{7,6},{8,9},{9,8},{10,11... | collective-permute-start | bytes 2359304 | tf_op jit(solution)/shard_map/ppermute | solution.py:238
  126.5 13.4 %collective-permute-start.21 = (bf16[16,2,48,128]{3,2,1,0:T(8,128)(2,1)}, bf16[16,2,48,128]{3,2,1,0:T(8,128)(2,1)S(1)}, u32[]{:S(2)}, u32[]{:S(2)}) collective-permute-start(bf16[16,2,48,128]{3,2,1,0:T(8,128)(2,1)} %shard_map.103.refs_0_), channel_id=1, source_target_pairs={{0,2},{1,3},{2,4},{3,5},{4,6},{5,7},{6,0},{7,1},{8,10},{9,11},{10,... | collective-permute-start | bytes 1179656 | tf_op jit(solution)/shard_map/ppermute | solution.py:238
  128.0 11.9 %collective-permute-start.23 = (bf16[16,2,48,128]{3,2,1,0:T(8,128)(2,1)}, bf16[16,2,48,128]{3,2,1,0:T(8,128)(2,1)S(1)}, u32[]{:S(2)}, u32[]{:S(2)}) collective-permute-start(bf16[16,2,48,128]{3,2,1,0:T(8,128)(2,1)} %shard_map.103.refs_0_), channel_id=1, source_target_pairs={{0,6},{1,7},{2,0},{3,1},{4,2},{5,3},{6,4},{7,5},{8,14},{9,15},{10,... | collective-permute-start | bytes 1179656 | tf_op jit(solution)/shard_map/ppermute | solution.py:238
  130.0 10.0 %collective-permute-start.20 = (bf16[16,2,48,128]{3,2,1,0:T(8,128)(2,1)}, bf16[16,2,48,128]{3,2,1,0:T(8,128)(2,1)S(1)}, u32[]{:S(2)}, u32[]{:S(2)}) collective-permute-start(bf16[16,2,48,128]{3,2,1,0:T(8,128)(2,1)} %shard_map.103.refs_0_), channel_id=1, source_target_pairs={{0,1},{1,0},{2,3},{3,2},{4,5},{5,4},{6,7},{7,6},{8,9},{9,8},{10,11... | collective-permute-start | bytes 1179656 | tf_op jit(solution)/shard_map/ppermute | solution.py:238
  137.4 11.7 %collective-permute-start.16 = (bf16[16,2,48,128]{3,2,1,0:T(8,128)(2,1)}, bf16[16,2,48,128]{3,2,1,0:T(8,128)(2,1)}, u32[]{:S(2)}, u32[]{:S(2)}) collective-permute-start(bf16[16,2,48,128]{3,2,1,0:T(8,128)(2,1)} %shard_map.102.refs_0_), channel_id=1, source_target_pairs={{0,6},{1,7},{2,0},{3,1},{4,2},{5,3},{6,4},{7,5},{8,14},{9,15},{10,... | collective-permute-start | bytes 1179656 | tf_op jit(solution)/shard_map/ppermute | solution.py:238
  139.4 13.5 %collective-permute-start.14 = (bf16[16,2,48,128]{3,2,1,0:T(8,128)(2,1)}, bf16[16,2,48,128]{3,2,1,0:T(8,128)(2,1)}, u32[]{:S(2)}, u32[]{:S(2)}) collective-permute-start(bf16[16,2,48,128]{3,2,1,0:T(8,128)(2,1)} %shard_map.102.refs_0_), channel_id=1, source_target_pairs={{0,2},{1,3},{2,4},{3,5},{4,6},{5,7},{6,0},{7,1},{8,10},{9,11},{10,... | collective-permute-start | bytes 1179656 | tf_op jit(solution)/shard_map/ppermute | solution.py:238
  139.9 20.4 %collective-permute-start.25 = (bf16[16,2,48,128]{3,2,1,0:T(8,128)(2,1)S(1)}, bf16[16,2,48,128]{3,2,1,0:T(8,128)(2,1)S(1)}, u32[]{:S(2)}, u32[]{:S(2)}) collective-permute-start(bf16[16,2,48,128]{3,2,1,0:T(8,128)(2,1)S(1)} %collective-permute-done.21.refs_2_), channel_id=1, source_target_pairs={{0,2},{1,3},{2,4},{3,5},{4,6},{5,7},{6,0},{7,1},{8,10},{9,11},{10,... | collective-permute-start | bytes 1179656 | tf_op jit(solution)/shard_map/ppermute | solution.py:238
  139.9 20.4 %collective-permute-start.22 = (bf16[16,2,48,128]{3,2,1,0:T(8,128)(2,1)S(1)}, bf16[16,2,48,128]{3,2,1,0:T(8,128)(2,1)S(1)}, u32[]{:S(2)}, u32[]{:S(2)}) collective-permute-start(bf16[16,2,48,128]{3,2,1,0:T(8,128)(2,1)S(1)} %collective-permute-done.21.refs_2_), channel_id=1, source_target_pairs={{0,1},{1,0},{2,3},{3,2},{4,5},{5,4},{6,7},{7,6},{8,9},{9,8},{10,11... | collective-permute-start | bytes 1179656 | tf_op jit(solution)/shard_map/ppermute | solution.py:238
  140.0 20.7 %collective-permute-start.24 = (bf16[16,2,48,128]{3,2,1,0:T(8,128)(2,1)S(1)}, bf16[16,2,48,128]{3,2,1,0:T(8,128)(2,1)S(1)}, u32[]{:S(2)}, u32[]{:S(2)}) collective-permute-start(bf16[16,2,48,128]{3,2,1,0:T(8,128)(2,1)S(1)} %collective-permute-done.23.refs_4_), channel_id=1, source_target_pairs={{0,1},{1,0},{2,3},{3,2},{4,5},{5,4},{6,7},{7,6},{8,9},{9,8},{10,11... | collective-permute-start | bytes 1179656 | tf_op jit(solution)/shard_map/ppermute | solution.py:238
  149.1 12.0 %collective-permute-start.18 = (bf16[16,2,48,128]{3,2,1,0:T(8,128)(2,1)}, bf16[16,2,48,128]{3,2,1,0:T(8,128)(2,1)}, u32[]{:S(2)}, u32[]{:S(2)}) collective-permute-start(bf16[16,2,48,128]{3,2,1,0:T(8,128)(2,1)} %collective-permute-done.16.refs_4_), channel_id=1, source_target_pairs={{0,6},{1,7},{2,0},{3,1},{4,2},{5,3},{6,4},{7,5},{8,14},{9,15},{10,... | collective-permute-start | bytes 1179656 | tf_op jit(solution)/shard_map/ppermute | solution.py:238
  152.9 13.3 %collective-permute-start.13 = (bf16[16,2,48,128]{3,2,1,0:T(8,128)(2,1)}, bf16[16,2,48,128]{3,2,1,0:T(8,128)(2,1)}, u32[]{:S(2)}, u32[]{:S(2)}) collective-permute-start(bf16[16,2,48,128]{3,2,1,0:T(8,128)(2,1)} %shard_map.102.refs_0_), channel_id=1, source_target_pairs={{0,1},{1,0},{2,3},{3,2},{4,5},{5,4},{6,7},{7,6},{8,9},{9,8},{10,11... | collective-permute-start | bytes 1179656 | tf_op jit(solution)/shard_map/ppermute | solution.py:238
  160.3 1.9 collective-permute-start.26
  160.3 5.9 %collective-permute-start.17 = (bf16[16,2,48,128]{3,2,1,0:T(8,128)(2,1)}, bf16[16,2,48,128]{3,2,1,0:T(8,128)(2,1)}, u32[]{:S(2)}, u32[]{:S(2)}) collective-permute-start(bf16[16,2,48,128]{3,2,1,0:T(8,128)(2,1)} %collective-permute-done.16.refs_4_), channel_id=1, source_target_pairs={{0,1},{1,0},{2,3},{3,2},{4,5},{5,4},{6,7},{7,6},{8,9},{9,8},{10,11... | collective-permute-start | bytes 1179656 | tf_op jit(solution)/shard_map/ppermute | solution.py:238
  160.8 5.4 %collective-permute-start.15 = (bf16[16,2,48,128]{3,2,1,0:T(8,128)(2,1)}, bf16[16,2,48,128]{3,2,1,0:T(8,128)(2,1)}, u32[]{:S(2)}, u32[]{:S(2)}) collective-permute-start(bf16[16,2,48,128]{3,2,1,0:T(8,128)(2,1)} %collective-permute-done.14.refs_2_), channel_id=1, source_target_pairs={{0,1},{1,0},{2,3},{3,2},{4,5},{5,4},{6,7},{7,6},{8,9},{9,8},{10,11... | collective-permute-start | bytes 1179656 | tf_op jit(solution)/shard_map/ppermute | solution.py:238
  161.1 5.1 %collective-permute-start.19 = (bf16[16,2,48,128]{3,2,1,0:T(8,128)(2,1)}, bf16[16,2,48,128]{3,2,1,0:T(8,128)(2,1)}, u32[]{:S(2)}, u32[]{:S(2)}) collective-permute-start(bf16[16,2,48,128]{3,2,1,0:T(8,128)(2,1)} %collective-permute-done.18.refs_6_), channel_id=1, source_target_pairs={{0,1},{1,0},{2,3},{3,2},{4,5},{5,4},{6,7},{7,6},{8,9},{9,8},{10,11... | collective-permute-start | bytes 1179656 | tf_op jit(solution)/shard_map/ppermute | solution.py:238
  170.2 49.7 %all-to-all-start.3 = ((bf16[32,2,48,256]{3,2,1,0:T(8,128)(2,1)}), bf16[32,2,48,256]{3,2,1,0:T(8,128)(2,1)S(1)}, u32[]{:S(2)}, u32[]{:S(2)}) async-start(bf16[32,2,48,256]{3,2,1,0:T(8,128)(2,1)} %shard_map.105), calls=%async_computation.3 | async-start | bytes 3145728 | tf_op jit(solution)/shard_map/all_to_all | solution.py:279
  (18 other events, 131.8 us)

commit v3 on v2

--- a/solution.py
+++ b/solution.py
@@ -76,7 +76,7 @@
 
 def dispatch(prompt, routes, tp_index, cap, experts, width):
     tokens, model_width = prompt.shape
-    parts = 4
+    parts = 2
     rows, block = tokens // parts, experts * cap // parts
     return pl.pallas_call(
         functools.partial(dispatch_kernel, cap),
@@ -146,37 +146,38 @@
     held, matrices, result, piece_sem, weight_sem, out_sem = refs[-6:]
     experts, count, cap, _ = held.shape
     width = pieces[0].shape[-1]
-    group = matrices.shape[1] // 8
     index = tp_ref[0]
 
+    weight_loads = [
+        pltpu.make_async_copy(weight_ref.at[:, e], matrices.at[e], weight_sem.at[e])
+        for e in range(experts)
+    ]
     loads = []
-    for e in range(experts):
-        for p in range(8):
-            dx, swap = PLACES[p]
-            source = (((index >> 1) + dx) & 3) * 2 + ((index & 1) ^ swap)
-            first = begin if pieces[p].shape[0] > count else 0
-            loads.append(
-                pltpu.make_async_copy(
-                    weight_ref.at[pl.ds(source * group, group), e],
-                    matrices.at[e, pl.ds(p * group, group)],
-                    weight_sem.at[e, p],
-                )
-            )
-            loads.append(
+    for p in range(8):
+        dx, swap = PLACES[p]
+        source = (((index >> 1) + dx) & 3) * 2 + ((index & 1) ^ swap)
+        first = begin if pieces[p].shape[0] > count else 0
+        loads.append(
+            [
                 pltpu.make_async_copy(
                     pieces[p].at[pl.ds(first, count), e],
-                    held.at[e, :, :, pl.ds(p * width, width)],
+                    held.at[e, :, :, pl.ds(pl.multiple_of(source * width, width), width)],
                     piece_sem.at[e, p],
                 )
-            )
-    for load in loads:
-        load.start()
+                for e in range(experts)
+            ]
+        )
+    for e in range(experts):
+        weight_loads[e].start()
+        for p in range(8):
+            loads[p][e].start()
 
     stores = []
     part = count // blocks
     for e in range(experts):
-        for load in loads[16 * e : 16 * e + 16]:
-            load.wait()
+        weight_loads[e].wait()
+        for p in range(8):
+            loads[p][e].wait()
         right = matrices[e].reshape(8 * width, matrices.shape[-1])
         for b in range(blocks):
             span = pl.ds(b * part, part)
@@ -222,7 +223,7 @@
             pltpu.VMEM((experts, sources) + weight.shape[2:], jnp.bfloat16),
             pltpu.VMEM((experts, count, cap, out_width), jnp.bfloat16),
             pltpu.SemaphoreType.DMA((experts, 8)),
-            pltpu.SemaphoreType.DMA((experts, 8)),
+            pltpu.SemaphoreType.DMA((experts,)),
             pltpu.SemaphoreType.DMA((experts,)),
         ],
         input_output_aliases=aliases,
@@ -300,7 +301,8 @@
     swapped = [piece for half in pieces for piece in half[1::2]]
     affinity = lax.optimization_barrier((affinity, *swapped))[0].T
     share = affinity / jnp.sum(affinity, axis=0, keepdims=True)
-    down = down_master.astype(jnp.bfloat16).reshape((fs_count, here) + down_master.shape[1:])
+    down = down_master.astype(jnp.bfloat16)
+    down = down.reshape((fs_count, here) + down_master.shape[1:])
     gate_up_new = exchange(gate_up)
     down_new = exchange(down)
     hidden = [

time: 223 us -> 222 us (level)
  transfers between devices with their start and end apart: 31 -> 31, of which waited for: 13 -> 13; matrix products, arithmetic and copies ran while one was open for 5% -> 5% of each run, Pallas kernels for 7% -> 6%
where the time goes in v3:
time: 222 us
  waiting for transfers between devices  129 us (58%)
  starting transfers between devices  52 us (23%)
  Pallas kernels  25.1 us (11%)
  local copies, waits for them, and re-layouts  9.35 us (4%)
  other arithmetic  5.69 us (3%)
    all_to_all x4, waiting for transfers between devices, exchange(): return lax.all_to_all(array, 'fs', split_axis=0, concat_axis=0, tiled=True)  76.2 us
    ppermute x27, waiting for transfers between devices, move(): return lax.ppermute(array, 'tp', tp_move(dx, swap))  52.4 us
    all_to_all x4, starting transfers between devices, exchange(): return lax.all_to_all(array, 'fs', split_axis=0, concat_axis=0, tiled=True)  33.3 us
    ppermute x27, starting transfers between devices, move(): return lax.ppermute(array, 'tp', tp_move(dx, swap))  18.6 us
    pallas_call x4, Pallas kernels, expert_matmul(): pl.pallas_call(functools.partial(expert_matmul_kernel, gated, blocks, hal...  17.9 us
    transpose x4, local copies, waits for them, and re-layouts, rows_first(): return array.transpose(1, 0, 2, 3).reshape(here, -1, array.shape[-1])  4.84 us
    pallas_call x1, Pallas kernels, dispatch(): pl.pallas_call(functools.partial(dispatch_kernel, cap), in_specs=[pl.Bloc...  4.57 us
  transfers between devices with their start and end apart: 31, of which 13 were waited for; matrix products, arithmetic and copies ran while one was open for 5% of the time, Pallas kernels for 6%

profile of v3, /device:TPU:16, one launch (start us, length us, event | category | flops | bytes accessed | tf_op | source)
XLA Modules:
  0.0 221.7 jit_solution(13561294232709528721)
XLA Ops:
  1.3 4.6 %dispatch.1 = (bf16[3072,256]{1,0:T(8,128)(2,1)}, s32[2,768]{1,0:T(2,128)S(1)}) custom-call(s32[1]{0:T(128)} %bitcast.tp_ref, s32[2,768]{1,0:T(2,128)S(1)} %bitcast.17, bf16[768,2048]{1,0:T(8,128)(2,1)} %prompt_ref.1), custom_call_target="tpu_custom_call" | custom-call | tf_op jit(solution)/shard_map/dispatch/pallas_call | solution.py:81
  5.9 11.6 %all-to-all-start = ((bf16[32,2,48,256]{3,2,1,0:T(8,128)(2,1)}), bf16[32,2,48,256]{3,2,1,0:T(8,128)(2,1)S(1)}, u32[]{:S(2)}, u32[]{:S(2)}) async-start(bf16[32,2,48,256]{3,2,1,0:T(8,128)(2,1)} %bitcast.21), calls=%async_computation | async-start | bytes 3145728 | tf_op jit(solution)/shard_map/all_to_all | solution.py:280
  17.5 2.9 %multiply_convert_fusion.1 = (bf16[64,64,128]{2,1,0:T(8,128)(2,1)S(1)}, bf16[64,64,128]{2,1,0:T(8,128)(2,1)S(1)}) fusion(f32[64,64,128]{2,1,0:T(8,128)} %param.11, f32[64]{0:T(128)S(1)} %copy-done.18, f32[64,64,128]{2,1,0:T(8,128)} %param.12), kind=kLoop, calls=%fused_computation.2 | loop fusion | flops 2097152 | bytes 6291712 | tf_op jit(solution)/shard_map/convert_element_type | solution.py:298
  20.4 1.7 pad_maximum_fusion
  22.1 34.7 %all-to-all-done.refs_0_ = bf16[32,2,48,256]{3,2,1,0:T(8,128)(2,1)S(1)} async-done(((bf16[32,2,48,256]{3,2,1,0:T(8,128)(2,1)}), bf16[32,2,48,256]{3,2,1,0:T(8,128)(2,1)S(1)}, u32[]{:S(2)}, u32[]{:S(2)}) %all-to-all-start) | async-done | bytes 1572896 | tf_op jit(solution)/shard_map/all_to_all | solution.py:280
  56.8 5.6 %all-to-all-start.1 = ((bf16[32,2,64,256]{3,2,1,0:T(8,128)(2,1)}), bf16[32,2,64,256]{3,2,1,0:T(8,128)(2,1)}, u32[]{:S(2)}, u32[]{:S(2)}) async-start(bf16[32,2,64,256]{3,2,1,0:T(8,128)(2,1)} %bitcast.19), calls=%async_computation.1 | async-start | bytes 4194304 | tf_op jit(solution)/shard_map/all_to_all | solution.py:280
  62.6 1.6 collective-permute-start.1
  64.1 1.8 collective-permute-start.3
  65.9 1.6 collective-permute-start.9
  67.9 16.5 %collective-permute-done.1.refs_2_ = bf16[16,2,48,256]{3,2,1,0:T(8,128)(2,1)} collective-permute-done((bf16[16,2,48,256]{3,2,1,0:T(8,128)(2,1)S(1)}, bf16[16,2,48,256]{3,2,1,0:T(8,128)(2,1)}, u32[]{:S(2)}, u32[]{:S(2)}) %collective-permute-start.1) | collective-permute-done | bytes 786464 | tf_op jit(solution)/shard_map/ppermute | solution.py:239
  84.7 13.6 %collective-permute-done.9.refs_4_ = bf16[16,2,48,256]{3,2,1,0:T(8,128)(2,1)S(1)} collective-permute-done((bf16[16,2,48,256]{3,2,1,0:T(8,128)(2,1)S(1)}, bf16[16,2,48,256]{3,2,1,0:T(8,128)(2,1)S(1)}, u32[]{:S(2)}, u32[]{:S(2)}) %collective-permute-start.9) | collective-permute-done | bytes 786464 | tf_op jit(solution)/shard_map/ppermute | solution.py:239
  98.3 2.8 %collective-permute-done.7.refs_2_ = bf16[16,2,48,256]{3,2,1,0:T(8,128)(2,1)S(1)} collective-permute-done((bf16[16,2,48,256]{3,2,1,0:T(8,128)(2,1)S(1)}, bf16[16,2,48,256]{3,2,1,0:T(8,128)(2,1)S(1)}, u32[]{:S(2)}, u32[]{:S(2)}) %collective-permute-start.7) | collective-permute-done | bytes 786464 | tf_op jit(solution)/shard_map/ppermute | solution.py:239
  102.0 1.6 collective-permute-start.11
  103.6 1.1 convert_element_type.11
  104.7 6.5 %all-to-all-done.1.refs_8_ = bf16[32,2,64,256]{3,2,1,0:T(8,128)(2,1)} async-done(((bf16[32,2,64,256]{3,2,1,0:T(8,128)(2,1)}), bf16[32,2,64,256]{3,2,1,0:T(8,128)(2,1)}, u32[]{:S(2)}, u32[]{:S(2)}) %all-to-all-start.1) | async-done | bytes 2097184 | tf_op jit(solution)/shard_map/all_to_all | solution.py:280
  111.2 6.2 %all-to-all-start.2 = ((bf16[32,2,32,256]{3,2,1,0:T(8,128)(2,1)}), bf16[32,2,32,256]{3,2,1,0:T(8,128)(2,1)S(1)}, u32[]{:S(2)}, u32[]{:S(2)}) async-start(bf16[32,2,32,256]{3,2,1,0:T(8,128)(2,1)} %bitcast.20), calls=%async_computation.2 | async-start | bytes 2097152 | tf_op jit(solution)/shard_map/all_to_all | solution.py:280
  118.3 1.2 collective-permute-done.11.refs_6_
  120.9 5.2 %shard_map.103.refs_0_ = bf16[16,2,48,128]{3,2,1,0:T(8,128)(2,1)} custom-call(s32[1]{0:T(128)} %bitcast.tp_ref, bf16[32,2,48,256]{3,2,1,0:T(8,128)(2,1)} %copy-done.1, bf16[32,2,48,256]{3,2,1,0:T(8,128)(2,1)} %collective-permute-done.refs_1_, bf16[16,2,48,256]{3,2,1,0:T(8,128)(2,1)} %collective-permute-done.1.refs_2_, ...), custom_call_target="tpu_custom_call" | custom-call | tf_op jit(solution)/shard_map/pallas_call | solution.py:214
  126.2 1.6 collective-permute-start.21
  127.7 2.0 collective-permute-start.23
  131.7 5.2 %shard_map.102.refs_0_ = bf16[16,2,48,128]{3,2,1,0:T(8,128)(2,1)} custom-call(s32[1]{0:T(128)} %bitcast.tp_ref, bf16[32,2,48,256]{3,2,1,0:T(8,128)(2,1)} %copy-done.1, bf16[32,2,48,256]{3,2,1,0:T(8,128)(2,1)} %collective-permute-done.refs_1_, bf16[16,2,48,256]{3,2,1,0:T(8,128)(2,1)} %copy-done.6, bf16[16,2,48,256]{3,2,1,0:T(8,128)(2,1)} %copy-done.8, ...), custom_call_target="tpu_custom_call" | custom-call | tf_op jit(solution)/shard_map/pallas_call | solution.py:214
  136.9 2.0 collective-permute-start.16
  140.2 8.4 %collective-permute-done.16.refs_4_ = bf16[16,2,48,128]{3,2,1,0:T(8,128)(2,1)} collective-permute-done((bf16[16,2,48,128]{3,2,1,0:T(8,128)(2,1)}, bf16[16,2,48,128]{3,2,1,0:T(8,128)(2,1)}, u32[]{:S(2)}, u32[]{:S(2)}) %collective-permute-start.16) | collective-permute-done | bytes 393248 | tf_op jit(solution)/shard_map/ppermute | solution.py:239
  148.6 3.1 %collective-permute-start.18 = (bf16[16,2,48,128]{3,2,1,0:T(8,128)(2,1)}, bf16[16,2,48,128]{3,2,1,0:T(8,128)(2,1)}, u32[]{:S(2)}, u32[]{:S(2)}) collective-permute-start(bf16[16,2,48,128]{3,2,1,0:T(8,128)(2,1)} %collective-permute-done.16.refs_4_), channel_id=1, source_target_pairs={{0,6},{1,7},{2,0},{3,1},{4,2},{5,3},{6,4},{7,5},{8,14},{9,15},{10,... | collective-permute-start | bytes 1179656 | tf_op jit(solution)/shard_map/ppermute | solution.py:239
  152.5 7.3 %collective-permute-done.25.refs_6_ = bf16[16,2,48,128]{3,2,1,0:T(8,128)(2,1)S(1)} collective-permute-done((bf16[16,2,48,128]{3,2,1,0:T(8,128)(2,1)S(1)}, bf16[16,2,48,128]{3,2,1,0:T(8,128)(2,1)S(1)}, u32[]{:S(2)}, u32[]{:S(2)}) %collective-permute-start.25) | collective-permute-done | bytes 393248 | tf_op jit(solution)/shard_map/ppermute | solution.py:239
  161.8 3.7 %shard_map.104.refs_9_ = bf16[32,2,48,256]{3,2,1,0:T(8,128)(2,1)} custom-call(s32[1]{0:T(128)} %bitcast.tp_ref, bf16[16,2,48,128]{3,2,1,0:T(8,128)(2,1)} %shard_map.103.refs_0_, bf16[16,2,48,128]{3,2,1,0:T(8,128)(2,1)} %copy-done.13, bf16[16,2,48,128]{3,2,1,0:T(8,128)(2,1)} %copy-done.11, bf16[16,2,48,128]{3,2,1,0:T(8,128)(2,1)} %copy-done.15, ...), custom_call_target="tpu_custom_call" | custom-call | tf_op jit(solution)/shard_map/pallas_call | solution.py:214
  165.5 3.7 %shard_map.105 = bf16[32,2,48,256]{3,2,1,0:T(8,128)(2,1)} custom-call(s32[1]{0:T(128)} %bitcast.tp_ref, bf16[16,2,48,128]{3,2,1,0:T(8,128)(2,1)} %shard_map.102.refs_0_, bf16[16,2,48,128]{3,2,1,0:T(8,128)(2,1)} %collective-permute-done.13.refs_1_, bf16[16,2,48,128]{3,2,1,0:T(8,128)(2,1)} %collective-permute-done.14.refs_2_, ...), custom_call_target="tpu_custom_call", output_to_operand_aliasing={{}: (10, {})} | custom-call | tf_op jit(solution)/shard_map/pallas_call | solution.py:214
  169.3 9.9 %all-to-all-start.3 = ((bf16[32,2,48,256]{3,2,1,0:T(8,128)(2,1)}), bf16[32,2,48,256]{3,2,1,0:T(8,128)(2,1)S(1)}, u32[]{:S(2)}, u32[]{:S(2)}) async-start(bf16[32,2,48,256]{3,2,1,0:T(8,128)(2,1)} %shard_map.105), calls=%async_computation.3 | async-start | bytes 3145728 | tf_op jit(solution)/shard_map/all_to_all | solution.py:280
  179.2 1.1 copy.14
  180.3 1.7 slice_bitcast_fusion
  184.1 34.9 %all-to-all-done.3 = bf16[32,2,48,256]{3,2,1,0:T(8,128)(2,1)S(1)} async-done(((bf16[32,2,48,256]{3,2,1,0:T(8,128)(2,1)}), bf16[32,2,48,256]{3,2,1,0:T(8,128)(2,1)S(1)}, u32[]{:S(2)}, u32[]{:S(2)}) %all-to-all-start.3) | async-done | bytes 1572896 | tf_op jit(solution)/shard_map/all_to_all | solution.py:280
  219.0 2.7 %combine.1 = bf16[768,256]{1,0:T(8,128)(2,1)} custom-call(s32[2,768]{1,0:T(2,128)S(1)} %get-tuple-element.7.slots_ref, f32[2,768]{1,0:T(2,128)S(1)} %divide_bitcast_fusion.share_ref, bf16[3072,256]{1,0:T(8,128)(2,1)S(1)} %bitcast.16), custom_call_target="tpu_custom_call" | custom-call | tf_op jit(solution)/shard_map/combine/pallas_call | solution.py:131
  (84 shorter events, 12.7 us)
Async XLA Ops:
  5.9 50.9 %all-to-all-start = ((bf16[32,2,48,256]{3,2,1,0:T(8,128)(2,1)}), bf16[32,2,48,256]{3,2,1,0:T(8,128)(2,1)S(1)}, u32[]{:S(2)}, u32[]{:S(2)}) async-start(bf16[32,2,48,256]{3,2,1,0:T(8,128)(2,1)} %bitcast.21), calls=%async_computation | async-start | bytes 3145728 | tf_op jit(solution)/shard_map/all_to_all | solution.py:280
  56.8 54.4 %all-to-all-start.1 = ((bf16[32,2,64,256]{3,2,1,0:T(8,128)(2,1)}), bf16[32,2,64,256]{3,2,1,0:T(8,128)(2,1)}, u32[]{:S(2)}, u32[]{:S(2)}) async-start(bf16[32,2,64,256]{3,2,1,0:T(8,128)(2,1)} %bitcast.19), calls=%async_computation.1 | async-start | bytes 4194304 | tf_op jit(solution)/shard_map/all_to_all | solution.py:280
  62.4 41.1 %copy-start.4 = (f32[64,32,256]{2,1,0:T(8,128)S(1)}, f32[64,32,256]{2,1,0:T(8,128)}, u32[]{:S(2)}) copy-start(f32[64,32,256]{2,1,0:T(8,128)} %param.13) | copy-start | bytes 6291460
  62.6 21.8 %collective-permute-start.1 = (bf16[16,2,48,256]{3,2,1,0:T(8,128)(2,1)S(1)}, bf16[16,2,48,256]{3,2,1,0:T(8,128)(2,1)}, u32[]{:S(2)}, u32[]{:S(2)}) collective-permute-start(bf16[16,2,48,256]{3,2,1,0:T(8,128)(2,1)S(1)} %get-tuple-element.13), channel_id=1, source_target_pairs={{0,2},{1,3},{2,4},{3,5},{4,6},{5,7},{6,0},{7,1},{8,10},{9,11},{10,... | collective-permute-start | bytes 2359304 | tf_op jit(solution)/shard_map/ppermute | solution.py:239
  64.1 20.5 %collective-permute-start.3 = (bf16[16,2,48,256]{3,2,1,0:T(8,128)(2,1)S(1)}, bf16[16,2,48,256]{3,2,1,0:T(8,128)(2,1)}, u32[]{:S(2)}, u32[]{:S(2)}) collective-permute-start(bf16[16,2,48,256]{3,2,1,0:T(8,128)(2,1)S(1)} %get-tuple-element.13), channel_id=1, source_target_pairs={{0,6},{1,7},{2,0},{3,1},{4,2},{5,3},{6,4},{7,5},{8,14},{9,15},{10,... | collective-permute-start | bytes 2359304 | tf_op jit(solution)/shard_map/ppermute | solution.py:239
  65.9 32.4 %collective-permute-start.9 = (bf16[16,2,48,256]{3,2,1,0:T(8,128)(2,1)S(1)}, bf16[16,2,48,256]{3,2,1,0:T(8,128)(2,1)S(1)}, u32[]{:S(2)}, u32[]{:S(2)}) collective-permute-start(bf16[16,2,48,256]{3,2,1,0:T(8,128)(2,1)S(1)} %get-tuple-element.12), channel_id=1, source_target_pairs={{0,6},{1,7},{2,0},{3,1},{4,2},{5,3},{6,4},{7,5},{8,14},{9,15},{10,... | collective-permute-start | bytes 2359304 | tf_op jit(solution)/shard_map/ppermute | solution.py:239
  67.4 33.7 %collective-permute-start.7 = (bf16[16,2,48,256]{3,2,1,0:T(8,128)(2,1)S(1)}, bf16[16,2,48,256]{3,2,1,0:T(8,128)(2,1)S(1)}, u32[]{:S(2)}, u32[]{:S(2)}) collective-permute-start(bf16[16,2,48,256]{3,2,1,0:T(8,128)(2,1)S(1)} %get-tuple-element.12), channel_id=1, source_target_pairs={{0,2},{1,3},{2,4},{3,5},{4,6},{5,7},{6,0},{7,1},{8,10},{9,11},{10,... | collective-permute-start | bytes 2359304 | tf_op jit(solution)/shard_map/ppermute | solution.py:239
  67.9 51.7 %collective-permute-start = (bf16[32,2,48,256]{3,2,1,0:T(8,128)(2,1)S(1)}, bf16[32,2,48,256]{3,2,1,0:T(8,128)(2,1)}, u32[]{:S(2)}, u32[]{:S(2)}) collective-permute-start(bf16[32,2,48,256]{3,2,1,0:T(8,128)(2,1)S(1)} %all-to-all-done.refs_0_), channel_id=1, source_target_pairs={{0,1},{1,0},{2,3},{3,2},{4,5},{5,4},{6,7},{7,6},{8,9},{9,8},{10,11... | collective-permute-start | bytes 4718600 | tf_op jit(solution)/shard_map/ppermute | solution.py:239
  84.4 33.1 %collective-permute-start.5 = (bf16[16,2,48,256]{3,2,1,0:T(8,128)(2,1)}, bf16[16,2,48,256]{3,2,1,0:T(8,128)(2,1)}, u32[]{:S(2)}, u32[]{:S(2)}) collective-permute-start(bf16[16,2,48,256]{3,2,1,0:T(8,128)(2,1)} %collective-permute-done.1.refs_2_), channel_id=1, source_target_pairs={{0,2},{1,3},{2,4},{3,5},{4,6},{5,7},{6,0},{7,1},{8,10},{9,11},{10,... | collective-permute-start | bytes 2359304 | tf_op jit(solution)/shard_map/ppermute | solution.py:239
  84.7 32.9 %collective-permute-start.2 = (bf16[16,2,48,256]{3,2,1,0:T(8,128)(2,1)}, bf16[16,2,48,256]{3,2,1,0:T(8,128)(2,1)}, u32[]{:S(2)}, u32[]{:S(2)}) collective-permute-start(bf16[16,2,48,256]{3,2,1,0:T(8,128)(2,1)} %collective-permute-done.1.refs_2_), channel_id=1, source_target_pairs={{0,1},{1,0},{2,3},{3,2},{4,5},{5,4},{6,7},{7,6},{8,9},{9,8},{10,11... | collective-permute-start | bytes 2359304 | tf_op jit(solution)/shard_map/ppermute | solution.py:239
  98.3 19.8 %collective-permute-start.4 = (bf16[16,2,48,256]{3,2,1,0:T(8,128)(2,1)}, bf16[16,2,48,256]{3,2,1,0:T(8,128)(2,1)}, u32[]{:S(2)}, u32[]{:S(2)}) collective-permute-start(bf16[16,2,48,256]{3,2,1,0:T(8,128)(2,1)} %collective-permute-done.3.refs_4_), channel_id=1, source_target_pairs={{0,1},{1,0},{2,3},{3,2},{4,5},{5,4},{6,7},{7,6},{8,9},{9,8},{10,11... | collective-permute-start | bytes 2359304 | tf_op jit(solution)/shard_map/ppermute | solution.py:239
  102.0 17.6 %collective-permute-start.11 = (bf16[16,2,48,256]{3,2,1,0:T(8,128)(2,1)S(1)}, bf16[16,2,48,256]{3,2,1,0:T(8,128)(2,1)}, u32[]{:S(2)}, u32[]{:S(2)}) collective-permute-start(bf16[16,2,48,256]{3,2,1,0:T(8,128)(2,1)S(1)} %collective-permute-done.9.refs_4_), channel_id=1, source_target_pairs={{0,6},{1,7},{2,0},{3,1},{4,2},{5,3},{6,4},{7,5},{8,14},{9,15},{10,... | collective-permute-start | bytes 2359304 | tf_op jit(solution)/shard_map/ppermute | solution.py:239
  111.2 49.6 %all-to-all-start.2 = ((bf16[32,2,32,256]{3,2,1,0:T(8,128)(2,1)}), bf16[32,2,32,256]{3,2,1,0:T(8,128)(2,1)S(1)}, u32[]{:S(2)}, u32[]{:S(2)}) async-start(bf16[32,2,32,256]{3,2,1,0:T(8,128)(2,1)} %bitcast.20), calls=%async_computation.2 | async-start | bytes 2097152 | tf_op jit(solution)/shard_map/all_to_all | solution.py:280
  117.5 2.6 %collective-permute-start.6 = (bf16[16,2,48,256]{3,2,1,0:T(8,128)(2,1)}, bf16[16,2,48,256]{3,2,1,0:T(8,128)(2,1)S(1)}, u32[]{:S(2)}, u32[]{:S(2)}) collective-permute-start(bf16[16,2,48,256]{3,2,1,0:T(8,128)(2,1)} %collective-permute-done.5.refs_6_), channel_id=1, source_target_pairs={{0,1},{1,0},{2,3},{3,2},{4,5},{5,4},{6,7},{7,6},{8,9},{9,8},{10,11... | collective-permute-start | bytes 2359304 | tf_op jit(solution)/shard_map/ppermute | solution.py:239
  117.6 12.1 %collective-permute-start.10 = (bf16[16,2,48,256]{3,2,1,0:T(8,128)(2,1)S(1)}, bf16[16,2,48,256]{3,2,1,0:T(8,128)(2,1)S(1)}, u32[]{:S(2)}, u32[]{:S(2)}) collective-permute-start(bf16[16,2,48,256]{3,2,1,0:T(8,128)(2,1)S(1)} %collective-permute-done.9.refs_4_), channel_id=1, source_target_pairs={{0,1},{1,0},{2,3},{3,2},{4,5},{5,4},{6,7},{7,6},{8,9},{9,8},{10,11... | collective-permute-start | bytes 2359304 | tf_op jit(solution)/shard_map/ppermute | solution.py:239
  118.1 11.9 %collective-permute-start.8 = (bf16[16,2,48,256]{3,2,1,0:T(8,128)(2,1)}, bf16[16,2,48,256]{3,2,1,0:T(8,128)(2,1)S(1)}, u32[]{:S(2)}, u32[]{:S(2)}) collective-permute-start(bf16[16,2,48,256]{3,2,1,0:T(8,128)(2,1)} %copy-done.6), channel_id=1, source_target_pairs={{0,1},{1,0},{2,3},{3,2},{4,5},{5,4},{6,7},{7,6},{8,9},{9,8},{10,11... | collective-permute-start | bytes 2359304 | tf_op jit(solution)/shard_map/ppermute | solution.py:239
  119.6 10.3 %collective-permute-start.12 = (bf16[16,2,48,256]{3,2,1,0:T(8,128)(2,1)}, bf16[16,2,48,256]{3,2,1,0:T(8,128)(2,1)S(1)}, u32[]{:S(2)}, u32[]{:S(2)}) collective-permute-start(bf16[16,2,48,256]{3,2,1,0:T(8,128)(2,1)} %collective-permute-done.11.refs_6_), channel_id=1, source_target_pairs={{0,1},{1,0},{2,3},{3,2},{4,5},{5,4},{6,7},{7,6},{8,9},{9,8},{10,11... | collective-permute-start | bytes 2359304 | tf_op jit(solution)/shard_map/ppermute | solution.py:239
  126.2 13.4 %collective-permute-start.21 = (bf16[16,2,48,128]{3,2,1,0:T(8,128)(2,1)}, bf16[16,2,48,128]{3,2,1,0:T(8,128)(2,1)S(1)}, u32[]{:S(2)}, u32[]{:S(2)}) collective-permute-start(bf16[16,2,48,128]{3,2,1,0:T(8,128)(2,1)} %shard_map.103.refs_0_), channel_id=1, source_target_pairs={{0,2},{1,3},{2,4},{3,5},{4,6},{5,7},{6,0},{7,1},{8,10},{9,11},{10,... | collective-permute-start | bytes 1179656 | tf_op jit(solution)/shard_map/ppermute | solution.py:239
  127.7 11.9 %collective-permute-start.23 = (bf16[16,2,48,128]{3,2,1,0:T(8,128)(2,1)}, bf16[16,2,48,128]{3,2,1,0:T(8,128)(2,1)S(1)}, u32[]{:S(2)}, u32[]{:S(2)}) collective-permute-start(bf16[16,2,48,128]{3,2,1,0:T(8,128)(2,1)} %shard_map.103.refs_0_), channel_id=1, source_target_pairs={{0,6},{1,7},{2,0},{3,1},{4,2},{5,3},{6,4},{7,5},{8,14},{9,15},{10,... | collective-permute-start | bytes 1179656 | tf_op jit(solution)/shard_map/ppermute | solution.py:239
  129.7 10.0 %collective-permute-start.20 = (bf16[16,2,48,128]{3,2,1,0:T(8,128)(2,1)}, bf16[16,2,48,128]{3,2,1,0:T(8,128)(2,1)S(1)}, u32[]{:S(2)}, u32[]{:S(2)}) collective-permute-start(bf16[16,2,48,128]{3,2,1,0:T(8,128)(2,1)} %shard_map.103.refs_0_), channel_id=1, source_target_pairs={{0,1},{1,0},{2,3},{3,2},{4,5},{5,4},{6,7},{7,6},{8,9},{9,8},{10,11... | collective-permute-start | bytes 1179656 | tf_op jit(solution)/shard_map/ppermute | solution.py:239
  136.9 11.7 %collective-permute-start.16 = (bf16[16,2,48,128]{3,2,1,0:T(8,128)(2,1)}, bf16[16,2,48,128]{3,2,1,0:T(8,128)(2,1)}, u32[]{:S(2)}, u32[]{:S(2)}) collective-permute-start(bf16[16,2,48,128]{3,2,1,0:T(8,128)(2,1)} %shard_map.102.refs_0_), channel_id=1, source_target_pairs={{0,6},{1,7},{2,0},{3,1},{4,2},{5,3},{6,4},{7,5},{8,14},{9,15},{10,... | collective-permute-start | bytes 1179656 | tf_op jit(solution)/shard_map/ppermute | solution.py:239
  139.0 13.5 %collective-permute-start.14 = (bf16[16,2,48,128]{3,2,1,0:T(8,128)(2,1)}, bf16[16,2,48,128]{3,2,1,0:T(8,128)(2,1)}, u32[]{:S(2)}, u32[]{:S(2)}) collective-permute-start(bf16[16,2,48,128]{3,2,1,0:T(8,128)(2,1)} %shard_map.102.refs_0_), channel_id=1, source_target_pairs={{0,2},{1,3},{2,4},{3,5},{4,6},{5,7},{6,0},{7,1},{8,10},{9,11},{10,... | collective-permute-start | bytes 1179656 | tf_op jit(solution)/shard_map/ppermute | solution.py:239
  139.6 20.2 %collective-permute-start.25 = (bf16[16,2,48,128]{3,2,1,0:T(8,128)(2,1)S(1)}, bf16[16,2,48,128]{3,2,1,0:T(8,128)(2,1)S(1)}, u32[]{:S(2)}, u32[]{:S(2)}) collective-permute-start(bf16[16,2,48,128]{3,2,1,0:T(8,128)(2,1)S(1)} %collective-permute-done.21.refs_2_), channel_id=1, source_target_pairs={{0,2},{1,3},{2,4},{3,5},{4,6},{5,7},{6,0},{7,1},{8,10},{9,11},{10,... | collective-permute-start | bytes 1179656 | tf_op jit(solution)/shard_map/ppermute | solution.py:239
  139.6 20.2 %collective-permute-start.22 = (bf16[16,2,48,128]{3,2,1,0:T(8,128)(2,1)S(1)}, bf16[16,2,48,128]{3,2,1,0:T(8,128)(2,1)S(1)}, u32[]{:S(2)}, u32[]{:S(2)}) collective-permute-start(bf16[16,2,48,128]{3,2,1,0:T(8,128)(2,1)S(1)} %collective-permute-done.21.refs_2_), channel_id=1, source_target_pairs={{0,1},{1,0},{2,3},{3,2},{4,5},{5,4},{6,7},{7,6},{8,9},{9,8},{10,11... | collective-permute-start | bytes 1179656 | tf_op jit(solution)/shard_map/ppermute | solution.py:239
  139.7 20.6 %collective-permute-start.24 = (bf16[16,2,48,128]{3,2,1,0:T(8,128)(2,1)S(1)}, bf16[16,2,48,128]{3,2,1,0:T(8,128)(2,1)S(1)}, u32[]{:S(2)}, u32[]{:S(2)}) collective-permute-start(bf16[16,2,48,128]{3,2,1,0:T(8,128)(2,1)S(1)} %collective-permute-done.23.refs_4_), channel_id=1, source_target_pairs={{0,1},{1,0},{2,3},{3,2},{4,5},{5,4},{6,7},{7,6},{8,9},{9,8},{10,11... | collective-permute-start | bytes 1179656 | tf_op jit(solution)/shard_map/ppermute | solution.py:239
  148.6 12.0 %collective-permute-start.18 = (bf16[16,2,48,128]{3,2,1,0:T(8,128)(2,1)}, bf16[16,2,48,128]{3,2,1,0:T(8,128)(2,1)}, u32[]{:S(2)}, u32[]{:S(2)}) collective-permute-start(bf16[16,2,48,128]{3,2,1,0:T(8,128)(2,1)} %collective-permute-done.16.refs_4_), channel_id=1, source_target_pairs={{0,6},{1,7},{2,0},{3,1},{4,2},{5,3},{6,4},{7,5},{8,14},{9,15},{10,... | collective-permute-start | bytes 1179656 | tf_op jit(solution)/shard_map/ppermute | solution.py:239
  152.5 13.0 %collective-permute-start.13 = (bf16[16,2,48,128]{3,2,1,0:T(8,128)(2,1)}, bf16[16,2,48,128]{3,2,1,0:T(8,128)(2,1)}, u32[]{:S(2)}, u32[]{:S(2)}) collective-permute-start(bf16[16,2,48,128]{3,2,1,0:T(8,128)(2,1)} %shard_map.102.refs_0_), channel_id=1, source_target_pairs={{0,1},{1,0},{2,3},{3,2},{4,5},{5,4},{6,7},{7,6},{8,9},{9,8},{10,11... | collective-permute-start | bytes 1179656 | tf_op jit(solution)/shard_map/ppermute | solution.py:239
  159.8 1.9 collective-permute-start.26
  159.8 5.7 %collective-permute-start.17 = (bf16[16,2,48,128]{3,2,1,0:T(8,128)(2,1)}, bf16[16,2,48,128]{3,2,1,0:T(8,128)(2,1)}, u32[]{:S(2)}, u32[]{:S(2)}) collective-permute-start(bf16[16,2,48,128]{3,2,1,0:T(8,128)(2,1)} %collective-permute-done.16.refs_4_), channel_id=1, source_target_pairs={{0,1},{1,0},{2,3},{3,2},{4,5},{5,4},{6,7},{7,6},{8,9},{9,8},{10,11... | collective-permute-start | bytes 1179656 | tf_op jit(solution)/shard_map/ppermute | solution.py:239
  160.3 5.2 %collective-permute-start.15 = (bf16[16,2,48,128]{3,2,1,0:T(8,128)(2,1)}, bf16[16,2,48,128]{3,2,1,0:T(8,128)(2,1)}, u32[]{:S(2)}, u32[]{:S(2)}) collective-permute-start(bf16[16,2,48,128]{3,2,1,0:T(8,128)(2,1)} %collective-permute-done.14.refs_2_), channel_id=1, source_target_pairs={{0,1},{1,0},{2,3},{3,2},{4,5},{5,4},{6,7},{7,6},{8,9},{9,8},{10,11... | collective-permute-start | bytes 1179656 | tf_op jit(solution)/shard_map/ppermute | solution.py:239
  160.7 4.9 %collective-permute-start.19 = (bf16[16,2,48,128]{3,2,1,0:T(8,128)(2,1)}, bf16[16,2,48,128]{3,2,1,0:T(8,128)(2,1)}, u32[]{:S(2)}, u32[]{:S(2)}) collective-permute-start(bf16[16,2,48,128]{3,2,1,0:T(8,128)(2,1)} %collective-permute-done.18.refs_6_), channel_id=1, source_target_pairs={{0,1},{1,0},{2,3},{3,2},{4,5},{5,4},{6,7},{7,6},{8,9},{9,8},{10,11... | collective-permute-start | bytes 1179656 | tf_op jit(solution)/shard_map/ppermute | solution.py:239
  169.3 49.7 %all-to-all-start.3 = ((bf16[32,2,48,256]{3,2,1,0:T(8,128)(2,1)}), bf16[32,2,48,256]{3,2,1,0:T(8,128)(2,1)S(1)}, u32[]{:S(2)}, u32[]{:S(2)}) async-start(bf16[32,2,48,256]{3,2,1,0:T(8,128)(2,1)} %shard_map.105), calls=%async_computation.3 | async-start | bytes 3145728 | tf_op jit(solution)/shard_map/all_to_all | solution.py:280
  (18 other events, 131.3 us)
